TPU v7x, 32 devices: a whole 2x2x4 slice. The times are simulated.
32 devices in a mesh: rep: 2 (over x), fs: 8 (over z, y), tp: 2 (over core).
Axes of the slice: x: 2, y: 2, z: 4, core: 2. Of those that a mesh axis runs over, the one named last changes fastest.
Arguments:
- tokens: bfloat16 [8192, 2048], P(('rep', 'fs', 'tp')), may hold values from -6 to 6
- norm_gain: float32 [2048], replicated, may hold values from 0.1 to 1.9
- gate_weight: float32 [2048, 5120], P('fs', 'tp'), may hold values from -0.125 to 0.125
- gate_scale: float32 [5120], P('tp'), may hold values from 0.1 to 1.9
- up_weight: float32 [2048, 5120], P('fs', 'tp'), may hold values from -0.125 to 0.125
- up_scale: float32 [5120], P('tp'), may hold values from 0.1 to 1.9
- down_weight: float32 [5120, 2048], P('tp', 'fs'), may hold values from -0.078125 to 0.078125
- down_scale: float32 [2048], replicated, may hold values from 0.1 to 1.9
Outputs:
- mixed: bfloat16 [8192, 2048], P(('rep', 'fs', 'tp'))
All inputs are finite; a program needn't handle non-finite values.
Results may differ from a plain program's by a relative error of at most 0.013.
Values may be sent and summed in bfloat16 or wider, within the bound.
A program may use at most 128 MiB of HBM per device.

v0:
```python
import functools

import jax
import jax.numpy as jnp
from jax import lax
from jax.experimental import pallas as pl
from jax.experimental.pallas import tpu as pltpu
from jax.sharding import PartitionSpec as P

EPS_VALUE = 1e-06


def from_partner(shard, axis, distance):
    return lax.ppermute(shard, axis, [(i, i ^ 1 << distance) for i in range(lax.axis_size(axis))])


def normalize(token_rows, norm_gain):
    values = token_rows.astype(jnp.float32)
    inverse = lax.rsqrt(jnp.mean(values * values, axis=-1, keepdims=True) + EPS_VALUE)
    return (values * inverse * norm_gain).astype(jnp.bfloat16)


def body(tokens, norm_gain, gate_weight, gate_scale, up_weight, up_scale, down_weight, down_scale):
    normed = normalize(tokens, norm_gain)
    gate_bf = gate_weight.astype(jnp.bfloat16)
    up_bf = up_weight.astype(jnp.bfloat16)
    down_bf = down_weight.astype(jnp.bfloat16)
    rep_index = lax.axis_index("rep")
    half_cols = gate_bf.shape[1] // 2
    half_rows = down_bf.shape[0] // 2
    own_gate = lax.dynamic_slice_in_dim(gate_bf, rep_index * half_cols, half_cols, 1)
    own_up = lax.dynamic_slice_in_dim(up_bf, rep_index * half_cols, half_cols, 1)
    own_down = lax.dynamic_slice_in_dim(down_bf, rep_index * half_rows, half_rows, 0)
    own_parts = (
        lax.all_gather(own_gate, "fs", axis=0, tiled=True),
        lax.all_gather(own_up, "fs", axis=0, tiled=True),
        lax.all_gather(own_down, "fs", axis=1, tiled=True),
    )
    far_parts = from_partner((own_parts[0], own_parts[1], own_parts[2]), "rep", 0)
    is_first = rep_index == 0

    def joined(own_part, far_part, axis_dim):
        return jnp.where(
            is_first,
            jnp.concatenate([own_part, far_part], axis_dim),
            jnp.concatenate([far_part, own_part], axis_dim),
        )

    gate_full = joined(own_parts[0], far_parts[0], 1)
    up_full = joined(own_parts[1], far_parts[1], 1)
    down_full = joined(own_parts[2], far_parts[2], 0)
    slab_rows = lax.all_gather(normed, "tp", axis=0, tiled=True)
    gate_pre = jnp.dot(slab_rows, gate_full, preferred_element_type=jnp.float32) * gate_scale
    up_pre = jnp.dot(slab_rows, up_full, preferred_element_type=jnp.float32) * up_scale
    hidden = (jax.nn.silu(gate_pre) * up_pre).astype(jnp.bfloat16)
    partial_value = (
        jnp.dot(hidden, down_full, preferred_element_type=jnp.float32) * down_scale
    ).astype(jnp.bfloat16)
    partial_value = lax.optimization_barrier(partial_value)
    return lax.psum_scatter(
        partial_value.astype(jnp.float32).astype(jnp.bfloat16),
        "tp",
        scatter_dimension=0,
        tiled=True,
    )


MESH = pl.DeviceIdType.MESH


def ffn_kernel(
    sizes, tok_ref, gain_ref, gate_ref, gscale_ref, up_ref, uscale_ref, down_ref, dscale_ref, out_ref,
    raw_g, raw_u, raw_d, wg, wu, wd, rows_x, acc_g, acc_u, hid, staged, landed,
    copy_sem, ring_send, ring_recv, down_send, down_recv, tok_send, tok_recv, part_send, part_recv,
):
    n_rep, n_fs, n_tp = sizes
    group = n_rep * n_tp
    steps = n_fs - 1
    half_ring = n_fs // 2
    n_tok, width = tok_ref.shape
    depth = wg.shape[1]
    half_depth = depth // 2
    cols = wd.shape[3]
    half_hid = wd.shape[2] // 2

    rep = lax.axis_index("rep")
    fs = lax.axis_index("fs")
    tp = lax.axis_index("tp")
    member = rep * n_tp + tp

    side = fs % 2
    place = (1 - side) * (fs // 2) + side * (n_fs - 1 - fs // 2)

    def fs_at(position):
        spot = (position + 2 * n_fs) % n_fs
        back = spot // half_ring
        return (1 - back) * 2 * spot + back * (2 * (n_fs - 1 - spot) + 1)

    right = (rep, fs_at(place + 1), tp)
    left = (rep, fs_at(place - 1), tp)

    def peer(offset):
        other = (member + offset) % group
        return other, (other // n_tp, fs, other % n_tp)

    def origin(direction, hops):
        return fs_at(place - hops) if direction == 0 else fs_at(place + hops)

    def ring_copy(direction, piece, step):
        store = wg if direction == 0 else wu
        part = store.at[origin(direction, step), pl.ds(piece * half_depth, half_depth)]
        return pltpu.make_async_remote_copy(
            src_ref=part, dst_ref=part,
            send_sem=ring_send.at[direction, piece, step], recv_sem=ring_recv.at[direction, piece, step],
            device_id=right if direction == 0 else left, device_id_type=MESH,
        )

    def ring_arrival(direction, piece, step):
        store = wg if direction == 0 else wu
        part = store.at[origin(direction, step + 1), pl.ds(piece * half_depth, half_depth)]
        return pltpu.make_async_remote_copy(
            src_ref=part, dst_ref=part,
            send_sem=ring_send.at[direction, piece, step], recv_sem=ring_recv.at[direction, piece, step],
            device_id=right if direction == 0 else left, device_id_type=MESH,
        )

    def down_copy(direction, piece, step, hops):
        part = wd.at[origin(direction, hops), direction, pl.ds(piece * half_hid, half_hid)]
        return pltpu.make_async_remote_copy(
            src_ref=part, dst_ref=part,
            send_sem=down_send.at[direction, piece, step], recv_sem=down_recv.at[direction, piece, step],
            device_id=right if direction == 0 else left, device_id_type=MESH,
        )

    def token_copy(offset, slot):
        return pltpu.make_async_remote_copy(
            src_ref=rows_x.at[slot], dst_ref=rows_x.at[slot],
            send_sem=tok_send.at[offset - 1], recv_sem=tok_recv.at[offset - 1],
            device_id=peer(offset)[1], device_id_type=MESH,
        )

    def part_copy(offset, index):
        other, where = peer(offset)
        return pltpu.make_async_remote_copy(
            src_ref=staged.at[index, other], dst_ref=landed.at[index, offset - 1],
            send_sem=part_send.at[index, offset - 1], recv_sem=part_recv.at[index, offset - 1],
            device_id=where, device_id_type=MESH,
        )

    units = pl.ds(pl.multiple_of(rep * wg.shape[2], 128), wg.shape[2])
    loads = []
    for piece in range(2):
        part = pl.ds(piece * half_depth, half_depth)
        for direction, source, store in ((0, gate_ref, raw_g), (1, up_ref, raw_u)):
            loads.append(
                pltpu.make_async_copy(source.at[part, units], store.at[part], copy_sem.at[2 * piece + direction])
            )
    loads.append(pltpu.make_async_copy(down_ref.at[units], raw_d, copy_sem.at[4]))
    for load in loads:
        load.start()
    barrier = pltpu.get_barrier_semaphore()
    for device in [right, left] + [peer(offset)[1] for offset in range(1, group)]:
        pl.semaphore_signal(barrier, inc=1, device_id=device, device_id_type=MESH)

    def round_piece(direction, piece):
        loads[2 * piece + direction].wait()
        part = slice(piece * half_depth, (piece + 1) * half_depth)
        raw, store = (raw_g, wg) if direction == 0 else (raw_u, wu)
        store[fs, part] = raw[part].astype(jnp.bfloat16)

    round_piece(0, 0)
    round_piece(1, 0)
    pl.semaphore_wait(barrier, group + 1)
    ring_copy(0, 0, 0).start()
    round_piece(0, 1)
    ring_copy(1, 0, 0).start()
    round_piece(1, 1)
    ring_copy(0, 1, 0).start()

    values = tok_ref[...].astype(jnp.float32)
    inverse = lax.rsqrt(jnp.mean(values * values, axis=-1, keepdims=True) + EPS_VALUE)
    rows_x[member] = (values * inverse * gain_ref[...]).astype(jnp.bfloat16)
    ring_copy(1, 1, 0).start()
    loads[4].wait()
    for direction in range(2):
        wd[fs, direction] = raw_d[:, direction * cols:(direction + 1) * cols].astype(jnp.bfloat16)
    for offset in range(1, group):
        token_copy(offset, member).start()

    def add_slice(index):
        gate_fs, up_fs = origin(0, index), origin(1, index)
        gate_cols = pl.ds(pl.multiple_of(gate_fs * depth, depth), depth)
        up_cols = pl.ds(pl.multiple_of(up_fs * depth, depth), depth)

        def tile(block, carry):
            gate_term = jnp.dot(rows_x[block, :, gate_cols], wg[gate_fs], preferred_element_type=jnp.float32)
            up_term = jnp.dot(rows_x[block, :, up_cols], wu[up_fs], preferred_element_type=jnp.float32)

            @pl.when(index == 0)
            def _():
                acc_g[block] = gate_term
                acc_u[block] = up_term

            @pl.when(index > 0)
            def _():
                acc_g[block] += gate_term
                acc_u[block] += up_term

            return carry

        lax.fori_loop(0, group, tile, 0)

    def ring_step(step, carry):
        @pl.when(step == steps - 3)
        def _():
            for piece in range(2):
                for direction in range(2):
                    down_copy(direction, piece, 0, 0).start()

        def both(piece, inner):
            for direction in range(2):
                ring_arrival(direction, piece, step).wait_recv()

                @pl.when(step < steps - 1)
                def _():
                    ring_copy(direction, piece, step + 1).start()

            @pl.when(step == steps - 1)
            def _():
                for direction in range(2):
                    down_copy(direction, piece, 0, 1).wait_recv()
                    down_copy(direction, piece, 1, 1).start()

            @pl.when((step == half_ring - 1) & (piece == 0))
            def _():
                for offset in range(1, group):
                    token_copy(offset, (member + group - offset) % group).wait_recv()

            @pl.when(step >= half_ring - 1)
            def _():
                add_slice(2 * (step - (half_ring - 1)) + piece)

            return inner

        return lax.fori_loop(0, 2, both, carry)

    lax.fori_loop(0, steps, ring_step, 0)

    def activate(block, carry):
        gate_pre = acc_g[block] * gscale_ref[:, units]
        up_pre = acc_u[block] * uscale_ref[:, units]
        hid[block] = (jax.nn.silu(gate_pre) * up_pre).astype(jnp.bfloat16)
        return carry

    lax.fori_loop(0, group, activate, 0)

    def produce(hops):
        for direction in range(2):
            source = origin(direction, hops)
            start = pl.multiple_of(source * 2 * cols + direction * cols, cols)
            scale = dscale_ref[:, pl.ds(start, cols)]
            index = 2 * hops + direction

            def tile(turn, carry):
                block = (member + 1 + turn) % group
                product = jnp.dot(hid[block], wd[source, direction], preferred_element_type=jnp.float32)
                staged[index, block] = (product * scale).astype(jnp.bfloat16)
                return carry

            lax.fori_loop(0, group, tile, 0)
            for offset in range(1, group):
                part_copy(offset, index).start()

    def down_step(step, carry):
        hops = step + 2
        for piece in range(2):
            for direction in range(2):
                down_copy(direction, piece, hops - 1, hops).wait_recv()

                @pl.when(hops < steps)
                def _():
                    down_copy(direction, piece, hops, hops).start()

        low = step + 2 * ((step // 2 + n_fs - 1) // n_fs)
        high = step + 1 + 2 * ((step + n_fs - 1) // n_fs)

        def one(done_hops, inner):
            produce(done_hops)
            return inner

        return lax.fori_loop(low, high, one, carry)

    lax.fori_loop(0, n_fs - 2, down_step, 0)

    def finish(hops, carry):
        for direction in range(2):
            index = 2 * hops + direction
            total = staged[index, member].astype(jnp.float32)
            for offset in range(1, group):
                part_copy(offset, index).wait_recv()
                total = total + landed[index, offset - 1].astype(jnp.float32)
            start = pl.multiple_of(origin(direction, hops) * 2 * cols + direction * cols, cols)
            out_ref[:, pl.ds(start, cols)] = total.astype(out_ref.dtype)
        return carry

    lax.fori_loop(0, n_fs, finish, 0)

    def drain(step, carry):
        for piece in range(2):
            for direction in range(2):
                ring_copy(direction, piece, step).wait_send()
                down_copy(direction, piece, step, step).wait_send()
        return carry

    lax.fori_loop(0, steps, drain, 0)

    def drain_parts(index, carry):
        for offset in range(1, group):
            part_copy(offset, index).wait_send()
        return carry

    lax.fori_loop(0, 2 * n_fs, drain_parts, 0)
    for offset in range(1, group):
        token_copy(offset, member).wait_send()


def kernel_body(sizes, tokens, norm_gain, gate_weight, gate_scale, up_weight, up_scale, down_weight, down_scale):
    n_rep, n_fs, n_tp = sizes
    group = n_rep * n_tp
    n_tok, width = tokens.shape
    depth = gate_weight.shape[0]
    units = gate_weight.shape[1] // n_rep
    cols = down_weight.shape[1] // 2
    vmem = pl.BlockSpec(memory_space=pltpu.VMEM)
    anywhere = pl.BlockSpec(memory_space=pl.ANY)
    steps = n_fs - 1
    bf = jnp.bfloat16
    dma = pltpu.SemaphoreType.DMA
    return pl.pallas_call(
        functools.partial(ffn_kernel, sizes),
        out_shape=jax.ShapeDtypeStruct((n_tok, width), bf),
        in_specs=[vmem, vmem, anywhere, vmem, anywhere, vmem, anywhere, vmem],
        out_specs=vmem,
        scratch_shapes=[
            pltpu.VMEM((depth, units), jnp.float32),
            pltpu.VMEM((depth, units), jnp.float32),
            pltpu.VMEM((units, 2 * cols), jnp.float32),
            pltpu.VMEM((n_fs, depth, units), bf),
            pltpu.VMEM((n_fs, depth, units), bf),
            pltpu.VMEM((n_fs, 2, units, cols), bf),
            pltpu.VMEM((group, n_tok, width), bf),
            pltpu.VMEM((group, n_tok, units), jnp.float32),
            pltpu.VMEM((group, n_tok, units), jnp.float32),
            pltpu.VMEM((group, n_tok, units), bf),
            pltpu.VMEM((2 * n_fs, group, n_tok, cols), bf),
            pltpu.VMEM((2 * n_fs, group - 1, n_tok, cols), bf),
            dma((5,)),
            dma((2, 2, steps)), dma((2, 2, steps)),
            dma((2, 2, steps)), dma((2, 2, steps)),
            dma((group - 1,)), dma((group - 1,)),
            dma((2 * n_fs, group - 1)), dma((2 * n_fs, group - 1)),
        ],
        compiler_params=pltpu.CompilerParams(
            collective_id=0, has_side_effects=True, vmem_limit_bytes=62 * 1024 * 1024
        ),
    )(
        tokens, norm_gain[None, :], gate_weight, gate_scale[None, :], up_weight, up_scale[None, :],
        down_weight, down_scale[None, :],
    )


def fits_kernel(mesh, tokens, gate_weight, down_weight):
    n_rep, n_fs, n_tp = (mesh.shape[name] for name in ("rep", "fs", "tp"))
    units = gate_weight.shape[1] // (n_tp * n_rep)
    aligned = units % 128 == 0 and down_weight.shape[1] // n_fs % 256 == 0
    return aligned and n_fs % 2 == 0 and n_fs >= 8 and n_rep * n_tp <= 4


def solution(mesh):
    sizes = tuple(mesh.shape[name] for name in ("rep", "fs", "tp"))

    def run(tokens, norm_gain, gate_weight, gate_scale, up_weight, up_scale, down_weight, down_scale):
        chosen = body
        if fits_kernel(mesh, tokens, gate_weight, down_weight):
            chosen = functools.partial(kernel_body, sizes)
        return jax.shard_map(
            chosen,
            mesh=mesh,
            in_specs=(
                P(("rep", "fs", "tp"), None),
                P(),
                P("fs", "tp"),
                P("tp"),
                P("fs", "tp"),
                P("tp"),
                P("tp", "fs"),
                P(),
            ),
            out_specs=P(("rep", "fs", "tp"), None),
            check_vma=False,
        )(tokens, norm_gain, gate_weight, gate_scale, up_weight, up_scale, down_weight, down_scale)

    return run
```

profile of v0, /device:TPU:17, one launch (start us, length us, event | category | flops | bytes accessed | tf_op | source)
XLA Modules:
  0.0 174.5 jit_solution(4668416480211982253)
XLA Ops:
  0.0 1.3 broadcast_in_dim.13.gscale_ref
  1.3 1.3 broadcast_in_dim.14.uscale_ref
  2.6 169.5 %shard_map.82 = bf16[256,2048]{1,0:T(8,128)(2,1)} custom-call(bf16[256,2048]{1,0:T(8,128)(2,1)} %tok_ref.1, f32[1,2048]{1,0:T(1,128)} %bitcast.2, f32[256,2560]{1,0:T(8,128)} %gate_ref.1, f32[1,2560]{1,0:T(1,128)} %broadcast_in_dim.13.gscale_ref, f32[256,2560]{1,0:T(8,128)} %up_ref.1, f32[1,2560]{1,0:T(1,128)} %broadcast_in_dim.14.uscale_ref, ...), custom_call_target="tpu_custom_call" | custom-call | tf_op jit(solution)/shard_map/pallas_call | solution.py:339
  172.2 2.3 %copy.10 = bf16[256,2048]{1,0:T(8,128)(2,1)} copy(bf16[256,2048]{1,0:T(8,128)(2,1)} %shard_map.82) | data formatting | bytes 2097152
where the time goes:
time: 175 us; the launch traced here: 174 us
  Pallas kernels  170 us (97%)
  local copies, waits for them, and re-layouts  4.92 us (3%)
    pallas_call x1, Pallas kernels, kernel_body(): pl.pallas_call(functools.partial(ffn_kernel, sizes), out_shape=jax.ShapeD...  170 us

commit v1 on v0

v1 whole, which is shorter than its diff:
```python
import functools

import jax
import jax.numpy as jnp
from jax import lax
from jax.experimental import pallas as pl
from jax.experimental.pallas import tpu as pltpu
from jax.sharding import PartitionSpec as P

EPS_VALUE = 1e-06


def from_partner(shard, axis, distance):
    return lax.ppermute(shard, axis, [(i, i ^ 1 << distance) for i in range(lax.axis_size(axis))])


def normalize(token_rows, norm_gain):
    values = token_rows.astype(jnp.float32)
    inverse = lax.rsqrt(jnp.mean(values * values, axis=-1, keepdims=True) + EPS_VALUE)
    return (values * inverse * norm_gain).astype(jnp.bfloat16)


def body(tokens, norm_gain, gate_weight, gate_scale, up_weight, up_scale, down_weight, down_scale):
    normed = normalize(tokens, norm_gain)
    gate_bf = gate_weight.astype(jnp.bfloat16)
    up_bf = up_weight.astype(jnp.bfloat16)
    down_bf = down_weight.astype(jnp.bfloat16)
    rep_index = lax.axis_index("rep")
    half_cols = gate_bf.shape[1] // 2
    half_rows = down_bf.shape[0] // 2
    own_gate = lax.dynamic_slice_in_dim(gate_bf, rep_index * half_cols, half_cols, 1)
    own_up = lax.dynamic_slice_in_dim(up_bf, rep_index * half_cols, half_cols, 1)
    own_down = lax.dynamic_slice_in_dim(down_bf, rep_index * half_rows, half_rows, 0)
    own_parts = (
        lax.all_gather(own_gate, "fs", axis=0, tiled=True),
        lax.all_gather(own_up, "fs", axis=0, tiled=True),
        lax.all_gather(own_down, "fs", axis=1, tiled=True),
    )
    far_parts = from_partner((own_parts[0], own_parts[1], own_parts[2]), "rep", 0)
    is_first = rep_index == 0

    def joined(own_part, far_part, axis_dim):
        return jnp.where(
            is_first,
            jnp.concatenate([own_part, far_part], axis_dim),
            jnp.concatenate([far_part, own_part], axis_dim),
        )

    gate_full = joined(own_parts[0], far_parts[0], 1)
    up_full = joined(own_parts[1], far_parts[1], 1)
    down_full = joined(own_parts[2], far_parts[2], 0)
    slab_rows = lax.all_gather(normed, "tp", axis=0, tiled=True)
    gate_pre = jnp.dot(slab_rows, gate_full, preferred_element_type=jnp.float32) * gate_scale
    up_pre = jnp.dot(slab_rows, up_full, preferred_element_type=jnp.float32) * up_scale
    hidden = (jax.nn.silu(gate_pre) * up_pre).astype(jnp.bfloat16)
    partial_value = (
        jnp.dot(hidden, down_full, preferred_element_type=jnp.float32) * down_scale
    ).astype(jnp.bfloat16)
    partial_value = lax.optimization_barrier(partial_value)
    return lax.psum_scatter(
        partial_value.astype(jnp.float32).astype(jnp.bfloat16),
        "tp",
        scatter_dimension=0,
        tiled=True,
    )


MESH = pl.DeviceIdType.MESH
DOWN = 4


def ffn_kernel(
    sizes, tok_ref, gain_ref, gate_ref, gscale_ref, up_ref, uscale_ref, down_ref, dscale_ref, out_ref,
    raw_gu, raw_d, wgu, wd, tgu, td, scales, rows, acc, hid, staged, landed_x, summed, landed_z,
    load_sem, scale_send, scale_recv, pair_send, mid_send, main_recv, thru_recv, y_send, y_recv, c_send, c_recv,
    tok_send, tok_recv, px_send, px_recv, pz_send, pz_recv,
):
    n_tok = tok_ref.shape[0]
    half_tok = n_tok // 2
    units = tgu.shape[3]
    depth = tgu.shape[2]
    half = depth // 2
    cols = wd.shape[2]

    rep = lax.axis_index("rep")
    fs = lax.axis_index("fs")
    tp = lax.axis_index("tp")
    z = fs // 2
    y = fs % 2
    side_z = z // 2
    inner = (z + side_z) % 2
    outer = 1 - inner
    is_inner = inner == 1
    is_outer = inner == 0
    z_pair = 1 + 4 * side_z - z

    pair_dev = (rep, z_pair * 2 + y, tp)
    mid_dev = (rep, (3 - z) * 2 + y, tp)
    y_dev = (rep, z * 2 + 1 - y, tp)
    x_dev = (1 - rep, fs, tp)
    c_dev = (rep, fs, 1 - tp)

    def remote(src, dst, send, recv, device):
        return pltpu.make_async_remote_copy(
            src_ref=src, dst_ref=dst, send_sem=send, recv_sem=recv, device_id=device, device_id_type=MESH
        )

    def shard_z(turn, own=z, other=z_pair):
        if isinstance(turn, int):
            return (own, other, 2 - side_z, 3 - 3 * side_z)[turn]
        late = turn // 2
        odd = turn % 2
        early = (1 - odd) * own + odd * other
        return (1 - late) * early + late * ((1 - odd) * (2 - side_z) + odd * (3 - 3 * side_z))

    def main_at(shard, shard_y, part, core):
        lanes = pl.ds(pl.multiple_of(core * units, 128), units)
        if isinstance(part, int) and part == DOWN:
            return wd.at[shard * 2 + shard_y, lanes]
        start = pl.multiple_of(shard_y * depth + (part % 2) * half, half)
        return wgu.at[part // 2, shard, pl.ds(start, half), lanes]

    def thru_at(turn, part):
        if isinstance(part, int) and part == DOWN:
            return td.at[turn]
        start = pl.multiple_of((part % 2) * half, half)
        return tgu.at[part // 2, turn, pl.ds(start, half)]

    def pair_copy(kind, part):
        send = pair_send.at[kind, part]
        if kind == 0:
            return remote(thru_at(0, part), main_at(z, y, part, tp), send, main_recv.at[1, part], pair_dev)
        if kind == 1:
            return remote(main_at(z, y, part, tp), thru_at(1, part), send, thru_recv.at[1, part], pair_dev)
        return remote(
            thru_at(kind, part), main_at(shard_z(kind), y, part, tp), send, main_recv.at[kind, part], pair_dev
        )

    def mid_copy(kind, part):
        send = mid_send.at[kind, part]
        turn = 2 + kind // 2
        if kind % 2 == 0:
            ref = main_at(shard_z(kind // 2), y, part, tp)
            return remote(ref, ref, send, main_recv.at[turn, part], mid_dev)
        return remote(thru_at(kind // 2, part), thru_at(turn, part), send, thru_recv.at[turn, part], mid_dev)

    def main_in(turn, part):
        ref = main_at(shard_z(turn), y, part, tp)
        return remote(ref, ref, pair_send.at[0, part], main_recv.at[turn, part], pair_dev)

    def thru_in(turn, part):
        ref = thru_at(turn, part)
        return remote(ref, ref, pair_send.at[0, part], thru_recv.at[turn, part], pair_dev)

    def y_copy(turn, part):
        ref = main_at(shard_z(turn), y, part, tp)
        return remote(ref, ref, y_send.at[turn, part], y_recv.at[turn, part], y_dev)

    def y_in(turn, part):
        ref = main_at(shard_z(turn), 1 - y, part, tp)
        return remote(ref, ref, y_send.at[turn, part], y_recv.at[turn, part], y_dev)

    def c_copy(turn, side, part):
        ref = main_at(shard_z(turn), y + side - 2 * side * y, part, tp)
        return remote(ref, ref, c_send.at[turn, side, part], c_recv.at[turn, side, part], c_dev)

    def c_in(turn, side, part):
        ref = main_at(shard_z(turn), y + side - 2 * side * y, part, 1 - tp)
        return remote(ref, ref, c_send.at[turn, side, part], c_recv.at[turn, side, part], c_dev)

    def tok_pair(piece):
        part = pl.ds(piece * half_tok, half_tok)
        return remote(
            rows.at[0, part], rows.at[1, part], tok_send.at[piece], tok_recv.at[piece], pair_dev
        )

    def tok_x():
        return remote(
            rows.at[0, pl.ds(0, n_tok)], rows.at[0, pl.ds(n_tok, n_tok)], tok_send.at[2], tok_recv.at[2], x_dev
        )

    def tok_far(piece):
        return remote(
            rows.at[1, pl.ds(piece * half_tok, half_tok)], rows.at[1, pl.ds(n_tok + piece * half_tok, half_tok)],
            tok_send.at[3 + piece], tok_recv.at[3 + piece], x_dev,
        )

    def part_x(block, far):
        return remote(
            staged.at[block, far, 1], landed_x.at[block, far], px_send.at[block, far], px_recv.at[block, far], x_dev
        )

    def part_z(block):
        return remote(summed.at[block], landed_z.at[block], pz_send.at[block], pz_recv.at[block], pair_dev)

    def scale_copy():
        return remote(scales.at[tp], scales.at[tp], scale_send, scale_recv, c_dev)

    def scale_in():
        return remote(scales.at[1 - tp], scales.at[1 - tp], scale_send, scale_recv, c_dev)

    base = rep * 2 * units
    both = pl.ds(pl.multiple_of(base, 128), 2 * units)
    loads = []
    for part in range(4):
        source = gate_ref if part // 2 == 0 else up_ref
        span = pl.ds((part % 2) * half, half)
        loads.append(
            pltpu.make_async_copy(source.at[span, both], raw_gu.at[part // 2, span], load_sem.at[part])
        )
    loads.append(pltpu.make_async_copy(down_ref.at[both], raw_d, load_sem.at[DOWN]))
    for load in loads:
        load.start()
    barrier = pltpu.get_barrier_semaphore()
    for device in (pair_dev, y_dev, x_dev, c_dev):
        pl.semaphore_signal(barrier, inc=1, device_id=device, device_id_type=MESH)

    @pl.when(is_inner)
    def _():
        pl.semaphore_signal(barrier, inc=1, device_id=mid_dev, device_id_type=MESH)

    mine = pl.ds(pl.multiple_of(outer * units, 128), units)
    theirs = pl.ds(pl.multiple_of(inner * units, 128), units)
    lanes = pl.ds(pl.multiple_of(tp * units, 128), units)

    def round_part(part):
        loads[part].wait()
        span = slice((part % 2) * half, (part % 2 + 1) * half)
        start = pl.multiple_of(y * depth + (part % 2) * half, half)
        wgu[part // 2, z, pl.ds(start, half), lanes] = raw_gu[part // 2, span, mine].astype(jnp.bfloat16)
        tgu[part // 2, 0, span] = raw_gu[part // 2, span, theirs].astype(jnp.bfloat16)

    def send_part(part):
        y_copy(0, part).start()
        pair_copy(0, part).start()

        @pl.when(is_inner)
        def _():
            mid_copy(0, part).start()

        c_copy(0, 0, part).start()

    round_part(0)
    pl.semaphore_wait(barrier, 4 + inner)
    send_part(0)
    values = tok_ref[...].astype(jnp.float32)
    inverse = lax.rsqrt(jnp.mean(values * values, axis=-1, keepdims=True) + EPS_VALUE)
    rows[0, :n_tok] = (values * inverse * gain_ref[...]).astype(jnp.bfloat16)
    tok_x().start()
    for part in range(1, 4):
        round_part(part)
        send_part(part)
    for piece in range(2):
        tok_pair(piece).start()

    @pl.when(is_inner)
    def _():
        for part in range(4):
            mid_copy(1, part).start()

    @pl.when(is_outer)
    def _():
        for part in range(4):
            pair_copy(1, part).start()

    unit_cols = pl.ds(pl.multiple_of(base + outer * units, 128), units)
    scales[tp, 0:1] = gscale_ref[:, unit_cols]
    scales[tp, 1:2] = uscale_ref[:, unit_cols]
    scale_copy().start()
    loads[DOWN].wait()
    wd[fs, lanes] = raw_d[pl.ds(pl.multiple_of(outer * units, 128), units)].astype(jnp.bfloat16)
    td[0] = raw_d[pl.ds(pl.multiple_of(inner * units, 128), units)].astype(jnp.bfloat16)
    c_copy(0, 0, DOWN).start()

    @pl.when(is_outer)
    def _():
        pair_copy(0, DOWN).start()
        pair_copy(1, DOWN).start()

    def take_main(turn, part):
        main_in(turn, part).wait_recv()
        y_copy(turn, part).start()
        c_copy(turn, 0, part).start()

    def take_y(turn, part):
        y_in(turn, part).wait_recv()
        c_copy(turn, 1, part).start()

    def each(count, step):
        def go(index, carry):
            step(index)
            return carry

        lax.fori_loop(0, count, go, 0)

    def first(part):
        take_main(1, part)

        @pl.when(is_inner)
        def _():
            mid_copy(2, part).start()

        take_y(0, part)

    each(4, first)

    @pl.when(is_inner)
    def _():
        each(4, lambda part: take_main(2, part))

    def second(part):
        @pl.when(is_inner)
        def _():
            thru_in(2, part).wait_recv()
            pair_copy(2, part).start()

        take_y(1, part)

    each(4, second)
    for piece in range(2):
        tok_pair(piece).wait_recv()
        tok_far(piece).start()

    @pl.when(is_inner)
    def _():
        def third(part):
            take_main(3, part)
            take_y(2, part)

        each(4, third)

    @pl.when(is_outer)
    def _():
        each(4, lambda part: take_main(2, part))

    def c_wait(turn):
        def go(index):
            c_in(turn, index // 4, index % 4).wait_recv()

        each(8, go)

    tok_x().wait_recv()
    c_wait(0)
    c_wait(1)

    @pl.when(is_inner)
    def _():
        c_wait(2)

    def term(far, matrix, turn):
        shard = shard_z(turn)
        span = pl.ds(pl.multiple_of(shard * 2 * depth, 2 * depth), 2 * depth)
        return jnp.dot(rows[far, :, span], wgu[matrix, shard], preferred_element_type=jnp.float32)

    def add_third(far, matrix, low, high):
        def go(turn, carry):
            acc[matrix, far] += term(far, matrix, turn)
            return carry

        lax.fori_loop(low, high, go, 0)

    def fourth(part):
        far, matrix = part // 2, part % 2

        @pl.when(is_inner)
        def _():
            thru_in(1, part).wait_recv()
            mid_copy(3, part).start()

        @pl.when(part == 2)
        def _():
            for piece in range(2):
                tok_far(piece).wait_recv()

        acc[matrix, far] = term(far, matrix, 0)
        acc[matrix, far] += term(far, matrix, 1)
        add_third(far, matrix, 2, 2 + inner)

        @pl.when(is_inner)
        def _():
            thru_in(3, part).wait_recv()
            pair_copy(3, part).start()
            take_y(3, part)

        @pl.when(is_outer)
        def _():
            take_y(2, part)
            take_main(3, part)

    each(4, fourth)
    y_copy(0, DOWN).start()

    @pl.when(is_inner)
    def _():
        mid_copy(0, DOWN).start()
        mid_copy(1, DOWN).start()
        pair_copy(0, DOWN).start()

    @pl.when(is_outer)
    def _():
        c_wait(2)

    def fifth(part):
        add_third(part // 2, part % 2, 2 + inner, 3)

        @pl.when(is_outer)
        def _():
            take_y(3, part)

    each(4, fifth)
    scale_in().wait_recv()
    c_wait(3)

    def activate(far):
        gate_scale = jnp.concatenate([scales[0, 0:1], scales[1, 0:1]], axis=1)
        up_scale = jnp.concatenate([scales[0, 1:2], scales[1, 1:2]], axis=1)
        gate_pre = (acc[0, far] + term(far, 0, 3)) * gate_scale
        up_pre = (acc[1, far] + term(far, 1, 3)) * up_scale
        hid[far] = (jax.nn.silu(gate_pre) * up_pre).astype(jnp.bfloat16)

    each(2, activate)

    def block_of(turn, side, own=z, other=z_pair):
        return shard_z(turn, own, other) * 2 + y + side - 2 * side * y

    def produce(block):
        start = pl.multiple_of(block * cols, cols)
        scale = dscale_ref[:, pl.ds(start, cols)]

        def tile(far):
            product = jnp.dot(hid[far], wd[block], preferred_element_type=jnp.float32) * scale
            staged[block, far] = product.astype(jnp.bfloat16).reshape(2, n_tok, cols)
            part_x(block, far).start()

        each(2, tile)

    def down_step(step):
        @pl.when((step >= 1) & (step < 4))
        def _():
            take_main(step, DOWN)

            @pl.when(is_inner)
            def _():
                thru_in(step, DOWN).wait_recv()

                @pl.when(step == 1)
                def _():
                    mid_copy(2, DOWN).start()
                    mid_copy(3, DOWN).start()

                @pl.when(step == 2)
                def _():
                    pair_copy(2, DOWN).start()

                @pl.when(step == 3)
                def _():
                    pair_copy(3, DOWN).start()

        def sides(side):
            turn = step - side

            @pl.when((turn >= 0) & (turn < 4))
            def _():
                @pl.when(side == 1)
                def _():
                    take_y(turn, DOWN)

                c_in(turn, side, DOWN).wait_recv()
                produce(block_of(turn, side))

        each(2, sides)

    each(5, down_step)

    def in_order(visit):
        def step_of(step):
            def sides(side):
                @pl.when((step - side >= 0) & (step - side < 4))
                def _():
                    visit(step - side, side)

            each(2, sides)

        each(5, step_of)

    def reduce_block(turn, side):
        block = block_of(turn, side)
        for far in (1, 0):
            part_x(block, far).wait_recv()
        total = staged[block, 1, 0].astype(jnp.float32) + landed_x[block, 1].astype(jnp.float32)
        summed[block] = total.astype(jnp.bfloat16)
        part_z(block).start()

    in_order(reduce_block)

    def finish(turn, side):
        block = block_of(turn, side, z_pair, z)
        part_z(block).wait_recv()
        total = staged[block, 0, 0].astype(jnp.float32) + landed_x[block, 0].astype(jnp.float32)
        total = total + landed_z[block].astype(jnp.float32)
        out_ref[:, pl.ds(pl.multiple_of(block * cols, cols), cols)] = total.astype(out_ref.dtype)

    in_order(finish)

    def drain_part(part):
        pair_copy(0, part).wait_send()

        @pl.when(is_outer)
        def _():
            pair_copy(1, part).wait_send()

        @pl.when(is_inner)
        def _():
            pair_copy(2, part).wait_send()
            pair_copy(3, part).wait_send()
            for kind in range(4):
                mid_copy(kind, part).wait_send()

        def turns(turn):
            y_copy(turn, part).wait_send()
            c_copy(turn, 0, part).wait_send()
            c_copy(turn, 1, part).wait_send()

        each(4, turns)

    each(4, drain_part)
    drain_part(DOWN)
    for piece in range(2):
        tok_pair(piece).wait_send()
        tok_far(piece).wait_send()
    tok_x().wait_send()
    scale_copy().wait_send()

    def drain_block(block):
        part_x(block, 0).wait_send()
        part_x(block, 1).wait_send()
        part_z(block).wait_send()

    each(8, drain_block)


def kernel_body(sizes, tokens, norm_gain, gate_weight, gate_scale, up_weight, up_scale, down_weight, down_scale):
    n_fs = sizes[1]
    n_tok, width = tokens.shape
    depth = gate_weight.shape[0]
    units = gate_weight.shape[1] // (2 * sizes[0])
    cols = down_weight.shape[1]
    vmem = pl.BlockSpec(memory_space=pltpu.VMEM)
    anywhere = pl.BlockSpec(memory_space=pl.ANY)
    bf, wide = jnp.bfloat16, jnp.float32
    dma = pltpu.SemaphoreType.DMA
    return pl.pallas_call(
        functools.partial(ffn_kernel, sizes),
        out_shape=jax.ShapeDtypeStruct((n_tok, width), bf),
        in_specs=[vmem, vmem, anywhere, vmem, anywhere, vmem, anywhere, vmem],
        out_specs=vmem,
        scratch_shapes=[
            pltpu.VMEM((2, depth, 2 * units), wide),
            pltpu.VMEM((2 * units, cols), wide),
            pltpu.VMEM((2, n_fs // 2, 2 * depth, 2 * units), bf),
            pltpu.VMEM((n_fs, 2 * units, cols), bf),
            pltpu.VMEM((2, 4, depth, units), bf),
            pltpu.VMEM((4, units, cols), bf),
            pltpu.VMEM((2, 2, units), wide),
            pltpu.VMEM((2, 2 * n_tok, width), bf),
            pltpu.VMEM((2, 2, 2 * n_tok, 2 * units), wide),
            pltpu.VMEM((2, 2 * n_tok, 2 * units), bf),
            pltpu.VMEM((n_fs, 2, 2, n_tok, cols), bf),
            pltpu.VMEM((n_fs, 2, n_tok, cols), bf),
            pltpu.VMEM((n_fs, n_tok, cols), bf),
            pltpu.VMEM((n_fs, n_tok, cols), bf),
            dma((5,)), dma, dma,
            dma((4, 5)), dma((4, 5)), dma((4, 5)), dma((4, 5)), dma((4, 5)), dma((4, 5)),
            dma((4, 2, 5)), dma((4, 2, 5)),
            dma((5,)), dma((5,)),
            dma((n_fs, 2)), dma((n_fs, 2)), dma((n_fs,)), dma((n_fs,)),
        ],
        compiler_params=pltpu.CompilerParams(
            collective_id=0, has_side_effects=True, vmem_limit_bytes=62 * 1024 * 1024
        ),
    )(
        tokens, norm_gain[None, :], gate_weight, gate_scale[None, :], up_weight, up_scale[None, :],
        down_weight, down_scale[None, :],
    )


def fits_kernel(mesh, tokens, gate_weight, down_weight):
    n_rep, n_fs, n_tp = (mesh.shape[name] for name in ("rep", "fs", "tp"))
    units = gate_weight.shape[1] // (n_tp * n_rep * 2)
    aligned = units % 128 == 0 and down_weight.shape[1] // n_fs % 128 == 0
    return aligned and n_rep == 2 and n_fs == 8 and n_tp == 2


def solution(mesh):
    sizes = tuple(mesh.shape[name] for name in ("rep", "fs", "tp"))

    def run(tokens, norm_gain, gate_weight, gate_scale, up_weight, up_scale, down_weight, down_scale):
        chosen = body
        if fits_kernel(mesh, tokens, gate_weight, down_weight):
            chosen = functools.partial(kernel_body, sizes)
        return jax.shard_map(
            chosen,
            mesh=mesh,
            in_specs=(
                P(("rep", "fs", "tp"), None),
                P(),
                P("fs", "tp"),
                P("tp"),
                P("fs", "tp"),
                P("tp"),
                P("tp", "fs"),
                P(),
            ),
            out_specs=P(("rep", "fs", "tp"), None),
            check_vma=False,
        )(tokens, norm_gain, gate_weight, gate_scale, up_weight, up_scale, down_weight, down_scale)

    return run
```

time: 175 us -> 148 us (0.85)
  Pallas kernels: 170 us -> 142 us
    pallas_call x1, Pallas kernels: 170 us -> 142 us  [kernel_body(): pl.pallas_call(functools.partial(ffn_kernel, sizes), out_shape=jax.ShapeD...]
where the time goes in v1:
time: 148 us; the launch traced here: 147 us
  Pallas kernels  142 us (96%)
  local copies, waits for them, and re-layouts  4.92 us (3%)
    pallas_call x1, Pallas kernels, kernel_body(): pl.pallas_call(functools.partial(ffn_kernel, sizes), out_shape=jax.ShapeD...  142 us

profile of v1, /device:TPU:17, one launch (start us, length us, event | category | flops | bytes accessed | tf_op | source)
XLA Modules:
  0.0 147.0 jit_solution(9284212436561440341)
XLA Ops:
  0.0 1.3 broadcast_in_dim.13.gscale_ref
  1.3 1.3 broadcast_in_dim.14.uscale_ref
  2.6 142.1 %shard_map.82 = bf16[256,2048]{1,0:T(8,128)(2,1)} custom-call(bf16[256,2048]{1,0:T(8,128)(2,1)} %tok_ref.1, f32[1,2048]{1,0:T(1,128)} %bitcast.2, f32[256,2560]{1,0:T(8,128)} %gate_ref.1, f32[1,2560]{1,0:T(1,128)} %broadcast_in_dim.13.gscale_ref, f32[256,2560]{1,0:T(8,128)} %up_ref.1, f32[1,2560]{1,0:T(1,128)} %broadcast_in_dim.14.uscale_ref, ...), custom_call_target="tpu_custom_call" | custom-call | tf_op jit(solution)/shard_map/pallas_call | solution.py:552
  144.7 2.3 %copy.10 = bf16[256,2048]{1,0:T(8,128)(2,1)} copy(bf16[256,2048]{1,0:T(8,128)(2,1)} %shard_map.82) | data formatting | bytes 2097152

commit v2 on v1

v2 whole, which is shorter than its diff:
```python
import functools

import jax
import jax.numpy as jnp
from jax import lax
from jax.experimental import pallas as pl
from jax.experimental.pallas import tpu as pltpu
from jax.sharding import PartitionSpec as P

EPS_VALUE = 1e-06


def from_partner(shard, axis, distance):
    return lax.ppermute(shard, axis, [(i, i ^ 1 << distance) for i in range(lax.axis_size(axis))])


def normalize(token_rows, norm_gain):
    values = token_rows.astype(jnp.float32)
    inverse = lax.rsqrt(jnp.mean(values * values, axis=-1, keepdims=True) + EPS_VALUE)
    return (values * inverse * norm_gain).astype(jnp.bfloat16)


def body(tokens, norm_gain, gate_weight, gate_scale, up_weight, up_scale, down_weight, down_scale):
    normed = normalize(tokens, norm_gain)
    gate_bf = gate_weight.astype(jnp.bfloat16)
    up_bf = up_weight.astype(jnp.bfloat16)
    down_bf = down_weight.astype(jnp.bfloat16)
    rep_index = lax.axis_index("rep")
    half_cols = gate_bf.shape[1] // 2
    half_rows = down_bf.shape[0] // 2
    own_gate = lax.dynamic_slice_in_dim(gate_bf, rep_index * half_cols, half_cols, 1)
    own_up = lax.dynamic_slice_in_dim(up_bf, rep_index * half_cols, half_cols, 1)
    own_down = lax.dynamic_slice_in_dim(down_bf, rep_index * half_rows, half_rows, 0)
    own_parts = (
        lax.all_gather(own_gate, "fs", axis=0, tiled=True),
        lax.all_gather(own_up, "fs", axis=0, tiled=True),
        lax.all_gather(own_down, "fs", axis=1, tiled=True),
    )
    far_parts = from_partner((own_parts[0], own_parts[1], own_parts[2]), "rep", 0)
    is_first = rep_index == 0

    def joined(own_part, far_part, axis_dim):
        return jnp.where(
            is_first,
            jnp.concatenate([own_part, far_part], axis_dim),
            jnp.concatenate([far_part, own_part], axis_dim),
        )

    gate_full = joined(own_parts[0], far_parts[0], 1)
    up_full = joined(own_parts[1], far_parts[1], 1)
    down_full = joined(own_parts[2], far_parts[2], 0)
    slab_rows = lax.all_gather(normed, "tp", axis=0, tiled=True)
    gate_pre = jnp.dot(slab_rows, gate_full, preferred_element_type=jnp.float32) * gate_scale
    up_pre = jnp.dot(slab_rows, up_full, preferred_element_type=jnp.float32) * up_scale
    hidden = (jax.nn.silu(gate_pre) * up_pre).astype(jnp.bfloat16)
    partial_value = (
        jnp.dot(hidden, down_full, preferred_element_type=jnp.float32) * down_scale
    ).astype(jnp.bfloat16)
    partial_value = lax.optimization_barrier(partial_value)
    return lax.psum_scatter(
        partial_value.astype(jnp.float32).astype(jnp.bfloat16),
        "tp",
        scatter_dimension=0,
        tiled=True,
    )


MESH = pl.DeviceIdType.MESH
DOWN = 4
PIECES = 4


def each(count, step):
    def go(index, carry):
        step(index)
        return carry

    lax.fori_loop(0, count, go, 0)


def ffn_kernel(
    tok_ref, gain_ref, gate_ref, gscale_ref, up_ref, uscale_ref, down_ref, dscale_ref, out_ref,
    tok, gain, gscale, uscale, dscale, raw_gu, raw_d, wgu, wd, tgu, td, scales, rows, acc, hid,
    staged, landed_x, summed, landed_z, landed_f, result,
    load_sem, out_sem, scale_send, scale_recv, pair_send, mid_send, main_recv, thru_recv, y_send, y_recv, c_send,
    c_recv, tok_send, tok_recv, px_send, px_recv, pz_send, pz_recv, pf_send, pf_recv,
):
    n_tok = tok.shape[0]
    piece_tok = n_tok // PIECES
    units = tgu.shape[3]
    depth = tgu.shape[2]
    half = depth // 2
    cols = wd.shape[2]

    rep = lax.axis_index("rep")
    fs = lax.axis_index("fs")
    tp = lax.axis_index("tp")
    z = fs // 2
    y = fs % 2
    side_z = z // 2
    inner = (z + side_z) % 2
    outer = 1 - inner
    is_inner = inner == 1
    is_outer = inner == 0
    z_pair = 1 + 4 * side_z - z

    pair_dev = (rep, z_pair * 2 + y, tp)
    mid_dev = (rep, (3 - z) * 2 + y, tp)
    y_dev = (rep, z * 2 + 1 - y, tp)
    x_dev = (1 - rep, fs, tp)
    c_dev = (rep, fs, 1 - tp)

    barrier = pltpu.get_barrier_semaphore()
    for device in (pair_dev, y_dev, x_dev, c_dev):
        pl.semaphore_signal(barrier, inc=1, device_id=device, device_id_type=MESH)

    @pl.when(is_inner)
    def _():
        pl.semaphore_signal(barrier, inc=1, device_id=mid_dev, device_id_type=MESH)

    def remote(src, dst, send, recv, device):
        return pltpu.make_async_remote_copy(
            src_ref=src, dst_ref=dst, send_sem=send, recv_sem=recv, device_id=device, device_id_type=MESH
        )

    def shard_z(turn):
        if isinstance(turn, int):
            return (z, z_pair, 2 - side_z, 3 - 3 * side_z)[turn]
        late = turn // 2
        odd = turn % 2
        early = (1 - odd) * z + odd * z_pair
        return (1 - late) * early + late * ((1 - odd) * (2 - side_z) + odd * (3 - 3 * side_z))

    def main_at(shard, shard_y, part, core):
        lanes = pl.ds(pl.multiple_of(core * units, 128), units)
        if isinstance(part, int) and part == DOWN:
            return wd.at[shard * 2 + shard_y, lanes]
        start = pl.multiple_of(shard_y * depth + (part % 2) * half, half)
        return wgu.at[part // 2, shard, pl.ds(start, half), lanes]

    def thru_at(turn, part):
        if isinstance(part, int) and part == DOWN:
            return td.at[turn]
        start = pl.multiple_of((part % 2) * half, half)
        return tgu.at[part // 2, turn, pl.ds(start, half)]

    def pair_copy(kind, part):
        send = pair_send.at[kind, part]
        if kind == 0:
            return remote(thru_at(0, part), main_at(z, y, part, tp), send, main_recv.at[1, part], pair_dev)
        if kind == 1:
            return remote(main_at(z, y, part, tp), thru_at(1, part), send, thru_recv.at[1, part], pair_dev)
        return remote(
            thru_at(kind, part), main_at(shard_z(kind), y, part, tp), send, main_recv.at[kind, part], pair_dev
        )

    def mid_copy(kind, part):
        send = mid_send.at[kind, part]
        turn = 2 + kind // 2
        if kind % 2 == 0:
            ref = main_at(shard_z(kind // 2), y, part, tp)
            return remote(ref, ref, send, main_recv.at[turn, part], mid_dev)
        return remote(thru_at(kind // 2, part), thru_at(turn, part), send, thru_recv.at[turn, part], mid_dev)

    def main_in(turn, part):
        ref = main_at(shard_z(turn), y, part, tp)
        return remote(ref, ref, pair_send.at[0, part], main_recv.at[turn, part], pair_dev)

    def thru_in(turn, part):
        ref = thru_at(turn, part)
        return remote(ref, ref, pair_send.at[0, part], thru_recv.at[turn, part], pair_dev)

    def y_copy(turn, part):
        ref = main_at(shard_z(turn), y, part, tp)
        return remote(ref, ref, y_send.at[turn, part], y_recv.at[turn, part], y_dev)

    def y_in(turn, part):
        ref = main_at(shard_z(turn), 1 - y, part, tp)
        return remote(ref, ref, y_send.at[turn, part], y_recv.at[turn, part], y_dev)

    def c_copy(turn, side, part):
        ref = main_at(shard_z(turn), y + side - 2 * side * y, part, tp)
        return remote(ref, ref, c_send.at[turn, side, part], c_recv.at[turn, side, part], c_dev)

    def c_in(turn, side, part):
        ref = main_at(shard_z(turn), y + side - 2 * side * y, part, 1 - tp)
        return remote(ref, ref, c_send.at[turn, side, part], c_recv.at[turn, side, part], c_dev)

    def tok_pair(piece):
        part = pl.ds(piece * piece_tok, piece_tok)
        return remote(
            rows.at[0, part], rows.at[1, part], tok_send.at[piece], tok_recv.at[piece], pair_dev
        )

    def tok_far(piece):
        return remote(
            rows.at[1, pl.ds(piece * piece_tok, piece_tok)],
            rows.at[1, pl.ds(n_tok + piece * piece_tok, piece_tok)],
            tok_send.at[PIECES + piece], tok_recv.at[PIECES + piece], x_dev,
        )

    def tok_x():
        return remote(
            rows.at[0, pl.ds(0, n_tok)], rows.at[0, pl.ds(n_tok, n_tok)],
            tok_send.at[2 * PIECES], tok_recv.at[2 * PIECES], x_dev,
        )

    def part_x(block, far):
        return remote(
            staged.at[block, far, 1], landed_x.at[block, far], px_send.at[block, far], px_recv.at[block, far], x_dev
        )

    def part_z(block):
        return remote(summed.at[block], landed_z.at[block], pz_send.at[block], pz_recv.at[block], pair_dev)

    def early_z(block):
        return remote(staged.at[block, 1, 0], landed_z.at[block], pz_send.at[block], pz_recv.at[block], pair_dev)

    def place_of(turn):
        late = turn // 2
        return (1 - late) * (shard_z(turn) - 2 * side_z) + 2 * late

    def early_far(block, place):
        return remote(
            staged.at[block, 1, 1], landed_f.at[place], pf_send.at[place], pf_recv.at[place], pair_dev
        )

    def scale_copy():
        return remote(scales.at[tp], scales.at[tp], scale_send, scale_recv, c_dev)

    def scale_in():
        return remote(scales.at[1 - tp], scales.at[1 - tp], scale_send, scale_recv, c_dev)

    base = rep * 2 * units
    both = pl.ds(pl.multiple_of(base, 128), 2 * units)
    loads = []
    for part in range(4):
        source = gate_ref if part // 2 == 0 else up_ref
        span = pl.ds((part % 2) * half, half)
        loads.append((source.at[span, both], raw_gu.at[part // 2, span]))
    loads.append((down_ref.at[both], raw_d))
    loads += [(tok_ref, tok), (gain_ref, gain), (gscale_ref, gscale), (uscale_ref, uscale), (dscale_ref, dscale)]
    loads = [pltpu.make_async_copy(*pair, load_sem.at[index]) for index, pair in enumerate(loads)]
    for index in (0, 5, 6, 1, 2, 3, 4, 7, 8, 9):
        loads[index].start()

    mine = pl.ds(pl.multiple_of(outer * units, 128), units)
    theirs = pl.ds(pl.multiple_of(inner * units, 128), units)
    lanes = pl.ds(pl.multiple_of(tp * units, 128), units)

    def round_part(part):
        loads[part].wait()
        span = slice((part % 2) * half, (part % 2 + 1) * half)
        start = pl.multiple_of(y * depth + (part % 2) * half, half)
        wgu[part // 2, z, pl.ds(start, half), lanes] = raw_gu[part // 2, span, mine].astype(jnp.bfloat16)
        tgu[part // 2, 0, span] = raw_gu[part // 2, span, theirs].astype(jnp.bfloat16)

    def send_part(part):
        pair_copy(0, part).start()
        y_copy(0, part).start()

        @pl.when(is_inner)
        def _():
            mid_copy(0, part).start()

        c_copy(0, 0, part).start()

    round_part(0)
    pl.semaphore_wait(barrier, 4 + inner)
    send_part(0)
    loads[5].wait()
    loads[6].wait()
    values = tok[...].astype(jnp.float32)
    inverse = lax.rsqrt(jnp.mean(values * values, axis=-1, keepdims=True) + EPS_VALUE)
    rows[0, :n_tok] = (values * inverse * gain[...]).astype(jnp.bfloat16)
    tok_x().start()
    for part in range(1, 4):
        round_part(part)
        send_part(part)
    for piece in range(PIECES):
        tok_pair(piece).start()

    @pl.when(is_inner)
    def _():
        for part in range(4):
            mid_copy(1, part).start()

    @pl.when(is_outer)
    def _():
        for part in range(4):
            pair_copy(1, part).start()

    for index in (7, 8, 9):
        loads[index].wait()
    first_row = (base + outer * units) // 128
    for index in range(units // 128):
        span = slice(index * 128, (index + 1) * 128)
        scales[tp, 0:1, span] = gscale[pl.ds(first_row + index, 1), :]
        scales[tp, 1:2, span] = uscale[pl.ds(first_row + index, 1), :]
    scale_copy().start()
    loads[DOWN].wait()
    wd[fs, lanes] = raw_d[mine].astype(jnp.bfloat16)
    td[0] = raw_d[theirs].astype(jnp.bfloat16)
    c_copy(0, 0, DOWN).start()

    @pl.when(is_outer)
    def _():
        pair_copy(0, DOWN).start()
        pair_copy(1, DOWN).start()

    def take_main(turn, part):
        main_in(turn, part).wait_recv()
        y_copy(turn, part).start()
        c_copy(turn, 0, part).start()

    def take_y(turn, part):
        y_in(turn, part).wait_recv()
        c_copy(turn, 1, part).start()

    def take_rows(piece):
        tok_pair(piece).wait_recv()
        tok_far(piece).start()

    def c_wait(turn):
        each(8, lambda index: c_in(turn, index // 4, index % 4).wait_recv())

    def term(far, matrix, turn):
        shard = shard_z(turn)
        span = pl.ds(pl.multiple_of(shard * 2 * depth, 2 * depth), 2 * depth)
        return jnp.dot(rows[far, :, span], wgu[matrix, shard], preferred_element_type=jnp.float32)

    def add_early(part):
        far, matrix = part // 2, part % 2

        @pl.when(part == 2)
        def _():
            for piece in range(PIECES):
                tok_far(piece).wait_recv()

        acc[matrix, far] = term(far, matrix, 0)
        acc[matrix, far] += term(far, matrix, 1)

    def add_late(part):
        acc[part % 2, part // 2] += term(part // 2, part % 2, 2)

    def first(part):
        take_main(1, part)

        @pl.when(is_inner)
        def _():
            mid_copy(2, part).start()

        take_y(0, part)

    each(4, first)

    @pl.when(is_inner)
    def _():
        each(4, lambda part: take_main(2, part))

    @pl.when(is_outer)
    def _():
        y_copy(0, DOWN).start()

    def second(part):
        @pl.when(is_inner)
        def _():
            thru_in(2, part).wait_recv()
            pair_copy(2, part).start()

        take_y(1, part)

        @pl.when((part == 1) | (part == 2))
        def _():
            take_rows(part - 1)

    each(4, second)
    take_rows(2)

    def pass_outward(part):
        thru_in(1, part).wait_recv()
        mid_copy(3, part).start()

    @pl.when(is_inner)
    def _():
        def third(part):
            take_main(3, part)
            take_y(2, part)

            @pl.when(part == 1)
            def _():
                take_rows(3)

            @pl.when(part == 2)
            def _():
                pass_outward(0)

        each(4, third)
        y_copy(0, DOWN).start()

    @pl.when(is_outer)
    def _():
        take_rows(3)

    tok_x().wait_recv()
    c_wait(0)
    c_wait(1)

    @pl.when(is_inner)
    def _():
        c_wait(2)

        def fourth(part):
            @pl.when(part < 3)
            def _():
                pass_outward(part + 1)

            @pl.when(part == 2)
            def _():
                mid_copy(1, DOWN).start()
                mid_copy(0, DOWN).start()

            add_early(part)
            add_late(part)
            thru_in(3, part).wait_recv()
            pair_copy(3, part).start()
            take_y(3, part)

        each(4, fourth)
        pair_copy(0, DOWN).start()

    @pl.when(is_outer)
    def _():
        def fourth(part):
            take_main(2, part)

            @pl.when(part > 0)
            def _():
                take_y(2, part - 1)

            add_early(part)

        each(4, fourth)

        def fifth(part):
            take_main(3, part)

            @pl.when(part == 0)
            def _():
                take_y(2, 3)
                c_wait(2)

            @pl.when(part > 0)
            def _():
                take_y(3, part - 1)

            add_late(part)

        each(4, fifth)
        take_y(3, 3)
        take_y(0, DOWN)
        c_in(0, 1, DOWN).wait_recv()

    def block_of(turn, side):
        return shard_z(turn) * 2 + y + side - 2 * side * y

    def z_first(turn, side):
        return ((side == 1) & (turn < 2)) | ((side == 0) & (turn == 2))

    def send_off(turn, side, far, near_x):
        block = block_of(turn, side)
        ahead = z_first(turn, side)
        crossing = far + inner == 1

        @pl.when((near_x == 1) & (jnp.logical_not(ahead) | jnp.logical_not(crossing)))
        def _():
            part_x(block, far).start()

        @pl.when(ahead & crossing & is_outer)
        def _():
            @pl.when(near_x == 1)
            def _():
                early_far(block, place_of(turn)).start()

            @pl.when(near_x == 0)
            def _():
                early_z(block).start()

    def scale_of(block):
        return dscale[:, pl.ds(pl.multiple_of(block * cols, cols), cols)]

    scale_in().wait_recv()
    c_wait(3)
    c_in(0, 0, DOWN).wait_recv()

    def activate(index):
        swap = (index + 1) // 2 % 2
        far = inner + swap - 2 * inner * swap
        near_x = 1 - index // 2
        span = pl.ds(pl.multiple_of(near_x * n_tok, n_tok), n_tok)
        shard = shard_z(3)
        depths = pl.ds(pl.multiple_of(shard * 2 * depth, 2 * depth), 2 * depth)
        pre = []
        for matrix in range(2):
            last = jnp.dot(rows[far, span, depths], wgu[matrix, shard], preferred_element_type=jnp.float32)
            scale = jnp.concatenate(
                [scales[0, matrix:matrix + 1], scales[1, matrix:matrix + 1]], axis=1
            )
            pre.append((acc[matrix, far, span] + last) * scale)
        hid[far, span] = (jax.nn.silu(pre[0]) * pre[1]).astype(jnp.bfloat16)

        def one(side, carry):
            block = block_of(0, side)
            product = jnp.dot(hid[far, span], wd[block], preferred_element_type=jnp.float32) * scale_of(block)
            staged[block, far, near_x] = product.astype(jnp.bfloat16)
            send_off(0, side, far, near_x)
            return carry

        lax.fori_loop(0, 1 + outer, one, 0)

    each(4, activate)

    def produce(turn, side):
        block = block_of(turn, side)

        def tile(index):
            far = 1 - index
            product = jnp.dot(hid[far], wd[block], preferred_element_type=jnp.float32) * scale_of(block)
            staged[block, far] = product.astype(jnp.bfloat16).reshape(2, n_tok, cols)
            for near_x in (1, 0):
                send_off(turn, side, far, near_x)

        each(2, tile)

    def fold(turn, side):
        block = block_of(turn, side)

        @pl.when(is_inner | jnp.logical_not(z_first(turn, side)))
        def _():
            part_x(block, 1).wait_recv()
            total = staged[block, 1, 0].astype(jnp.float32) + landed_x[block, 1].astype(jnp.float32)
            summed[block] = total.astype(jnp.bfloat16)
            part_z(block).start()

    def late_x(turn, side):
        block = block_of(turn, side)
        place = place_of(turn)
        early_far(block, place).wait_recv()
        total = staged[block, 0, 1].astype(jnp.float32) + landed_f[place].astype(jnp.float32)
        staged[block, 0, 1] = total.astype(jnp.bfloat16)
        part_x(block, 0).start()

    def down_step(index):
        step = index + 1
        swap = inner * (step // 3) * (1 - step // 4)

        @pl.when(is_inner & (step == 4))
        def _():
            late_x(0, 1)

        def sides(order):
            side = order + swap - 2 * order * swap
            turn = step - side

            @pl.when((turn < 4) & ((side == 0) | (turn > 0) | is_inner))
            def _():
                @pl.when(side == 0)
                def _():
                    take_main(turn, DOWN)

                @pl.when(side == 1)
                def _():
                    take_y(turn, DOWN)

                c_in(turn, side, DOWN).wait_recv()
                produce(turn, side)

        each(2, sides)

        @pl.when(is_inner)
        def _():
            @pl.when(step == 1)
            def _():
                thru_in(2, DOWN).wait_recv()
                pair_copy(2, DOWN).start()
                thru_in(1, DOWN).wait_recv()
                mid_copy(3, DOWN).start()
                mid_copy(2, DOWN).start()

            @pl.when(step == 2)
            def _():
                thru_in(3, DOWN).wait_recv()
                pair_copy(3, DOWN).start()

            @pl.when(step == 3)
            def _():
                late_x(1, 1)

        def folds(side):
            @pl.when(step - 1 - side >= 0)
            def _():
                fold(step - 1 - side, side)

        each(2, folds)

    each(4, down_step)
    fold(3, 1)

    @pl.when(is_inner)
    def _():
        late_x(2, 0)

    def out_copy(block):
        span = pl.ds(pl.multiple_of(block * cols, cols), cols)
        return pltpu.make_async_copy(result.at[:, span], out_ref.at[:, span], out_sem.at[block])

    def finish(index):
        block = block_of(outer * (index // 2) + inner * (3 - index // 2), index % 2)
        part_x(block, 0).wait_recv()
        part_z(block).wait_recv()
        total = staged[block, 0, 0].astype(jnp.float32) + landed_x[block, 0].astype(jnp.float32)
        total = total + landed_z[block].astype(jnp.float32)
        result[:, pl.ds(pl.multiple_of(block * cols, cols), cols)] = total.astype(result.dtype)
        out_copy(block).start()

    each(8, finish)

    def drain_part(part):
        pair_copy(0, part).wait_send()

        @pl.when(is_outer)
        def _():
            pair_copy(1, part).wait_send()

        @pl.when(is_inner)
        def _():
            pair_copy(2, part).wait_send()
            pair_copy(3, part).wait_send()
            for kind in range(4):
                mid_copy(kind, part).wait_send()

        def turns(turn):
            y_copy(turn, part).wait_send()
            c_copy(turn, 0, part).wait_send()
            c_copy(turn, 1, part).wait_send()

        each(4, turns)

    each(4, drain_part)
    drain_part(DOWN)

    def drain_rows(piece):
        tok_pair(piece).wait_send()
        tok_far(piece).wait_send()

    each(PIECES, drain_rows)
    tok_x().wait_send()
    scale_copy().wait_send()

    def drain_block(turn):
        def sides(side):
            block = block_of(turn, side)
            part_x(block, 0).wait_send()
            part_z(block).wait_send()
            ahead = z_first(turn, side)

            @pl.when(is_inner | jnp.logical_not(ahead))
            def _():
                part_x(block, 1).wait_send()

            @pl.when(is_outer & ahead)
            def _():
                early_far(block, place_of(turn)).wait_send()

            out_copy(block).wait()

        each(2, sides)

    each(4, drain_block)


def kernel_body(tokens, norm_gain, gate_weight, gate_scale, up_weight, up_scale, down_weight, down_scale, sizes):
    n_fs = sizes[1]
    n_tok, width = tokens.shape
    depth = gate_weight.shape[0]
    all_units = gate_weight.shape[1]
    units = all_units // (2 * sizes[0])
    cols = down_weight.shape[1]
    anywhere = pl.BlockSpec(memory_space=pl.ANY)
    bf, wide = jnp.bfloat16, jnp.float32
    dma = pltpu.SemaphoreType.DMA
    turns, parts = 4, 5
    return pl.pallas_call(
        ffn_kernel,
        out_shape=jax.ShapeDtypeStruct((n_tok, width), bf),
        in_specs=[anywhere] * 8,
        out_specs=anywhere,
        scratch_shapes=[
            pltpu.VMEM((n_tok, width), bf),
            pltpu.VMEM((1, width), wide),
            pltpu.VMEM((all_units // 128, 128), wide),
            pltpu.VMEM((all_units // 128, 128), wide),
            pltpu.VMEM((1, width), wide),
            pltpu.VMEM((2, depth, 2 * units), wide),
            pltpu.VMEM((2 * units, cols), wide),
            pltpu.VMEM((2, n_fs // 2, 2 * depth, 2 * units), bf),
            pltpu.VMEM((n_fs, 2 * units, cols), bf),
            pltpu.VMEM((2, turns, depth, units), bf),
            pltpu.VMEM((turns, units, cols), bf),
            pltpu.VMEM((2, 2, units), wide),
            pltpu.VMEM((2, 2 * n_tok, width), bf),
            pltpu.VMEM((2, 2, 2 * n_tok, 2 * units), wide),
            pltpu.VMEM((2, 2 * n_tok, 2 * units), bf),
            pltpu.VMEM((n_fs, 2, 2, n_tok, cols), bf),
            pltpu.VMEM((n_fs, 2, n_tok, cols), bf),
            pltpu.VMEM((n_fs, n_tok, cols), bf),
            pltpu.VMEM((n_fs, n_tok, cols), bf),
            pltpu.VMEM((3, n_tok, cols), bf),
            pltpu.VMEM((n_tok, width), bf),
            dma((10,)), dma((n_fs,)), dma, dma,
            dma((turns, parts)), dma((turns, parts)), dma((turns, parts)), dma((turns, parts)),
            dma((turns, parts)), dma((turns, parts)), dma((turns, 2, parts)), dma((turns, 2, parts)),
            dma((2 * PIECES + 1,)), dma((2 * PIECES + 1,)),
            dma((n_fs, 2)), dma((n_fs, 2)), dma((n_fs,)), dma((n_fs,)), dma((3,)), dma((3,)),
        ],
        compiler_params=pltpu.CompilerParams(
            collective_id=0, has_side_effects=True, vmem_limit_bytes=62 * 1024 * 1024
        ),
    )(
        tokens, norm_gain[None, :], gate_weight, gate_scale.reshape(-1, 128), up_weight, up_scale.reshape(-1, 128),
        down_weight, down_scale[None, :],
    )


def fits_kernel(mesh, tokens, gate_weight, down_weight):
    n_rep, n_fs, n_tp = (mesh.shape[name] for name in ("rep", "fs", "tp"))
    units = gate_weight.shape[1] // (n_tp * n_rep * 2)
    aligned = units % 128 == 0 and down_weight.shape[1] // n_fs % 128 == 0
    return aligned and n_rep == 2 and n_fs == 8 and n_tp == 2


def solution(mesh):
    sizes = tuple(mesh.shape[name] for name in ("rep", "fs", "tp"))

    def run(tokens, norm_gain, gate_weight, gate_scale, up_weight, up_scale, down_weight, down_scale):
        chosen = body
        if fits_kernel(mesh, tokens, gate_weight, down_weight):
            chosen = functools.partial(kernel_body, sizes=sizes)
        return jax.shard_map(
            chosen,
            mesh=mesh,
            in_specs=(
                P(("rep", "fs", "tp"), None),
                P(),
                P("fs", "tp"),
                P("tp"),
                P("fs", "tp"),
                P("tp"),
                P("tp", "fs"),
                P(),
            ),
            out_specs=P(("rep", "fs", "tp"), None),
            check_vma=False,
        )(tokens, norm_gain, gate_weight, gate_scale, up_weight, up_scale, down_weight, down_scale)

    return run
```

time: 148 us -> 126 us (0.85)
  Pallas kernels: 142 us -> 124 us
  local copies, waits for them, and re-layouts: 4.92 us -> 2.3 us
    pallas_call x1, Pallas kernels: 142 us -> 124 us  [kernel_body(): pl.pallas_call(ffn_kernel, out_shape=jax.ShapeDtypeStruct((n_tok, width),...]
    broadcast_in_dim x2 -> x0, local copies, waits for them, and re-layouts: 2.62 us -> none  [the longest x1 1.31 us: kernel_body(): gate_scale[None, :]]
where the time goes in v2:
time: 126 us
  Pallas kernels  124 us (98%)
  local copies, waits for them, and re-layouts  2.3 us (2%)
    pallas_call x1, Pallas kernels, kernel_body(): pl.pallas_call(ffn_kernel, out_shape=jax.ShapeDtypeStruct((n_tok, width),...  124 us

profile of v2, /device:TPU:17, one launch (start us, length us, event | category | flops | bytes accessed | tf_op | source)
XLA Modules:
  0.0 125.9 jit_solution(9119816428842190354)
XLA Ops:
  0.0 123.6 %shard_map.82 = bf16[256,2048]{1,0:T(8,128)(2,1)} custom-call(bf16[256,2048]{1,0:T(8,128)(2,1)} %tok_ref.1, f32[1,2048]{1,0:T(1,128)} %bitcast.6, f32[256,2560]{1,0:T(8,128)} %gate_ref.1, f32[20,128]{1,0:T(8,128)} %bitcast.4, f32[256,2560]{1,0:T(8,128)} %up_ref.1, f32[20,128]{1,0:T(8,128)} %bitcast.5, f32[2560,256]{1,0:T(8,128)} %down_ref.1, f32[1,2048]{1,0:T(1,128)} %bitcast.7), custom_call_target="tpu_custom_call" | custom-call | tf_op jit(solution)/shard_map/pallas_call | solution.py:693
  123.6 2.3 %copy.10 = bf16[256,2048]{1,0:T(8,128)(2,1)} copy(bf16[256,2048]{1,0:T(8,128)(2,1)} %shard_map.82) | data formatting | bytes 2097152

commit v3 on v2

--- a/solution.py
+++ b/solution.py
@@ -66,7 +66,8 @@
 
 
 MESH = pl.DeviceIdType.MESH
-DOWN = 4
+CUTS = 4
+DOWN = 2 * CUTS
 PIECES = 4
 
 
@@ -89,7 +90,7 @@
     piece_tok = n_tok // PIECES
     units = tgu.shape[3]
     depth = tgu.shape[2]
-    half = depth // 2
+    fine = depth // CUTS
     cols = wd.shape[2]
 
     rep = lax.axis_index("rep")
@@ -135,94 +136,102 @@
         lanes = pl.ds(pl.multiple_of(core * units, 128), units)
         if isinstance(part, int) and part == DOWN:
             return wd.at[shard * 2 + shard_y, lanes]
-        start = pl.multiple_of(shard_y * depth + (part % 2) * half, half)
-        return wgu.at[part // 2, shard, pl.ds(start, half), lanes]
+        start = pl.multiple_of(shard_y * depth + (part % CUTS) * fine, fine)
+        return wgu.at[part // CUTS, shard, pl.ds(start, fine), lanes]
 
     def thru_at(turn, part):
         if isinstance(part, int) and part == DOWN:
             return td.at[turn]
-        start = pl.multiple_of((part % 2) * half, half)
-        return tgu.at[part // 2, turn, pl.ds(start, half)]
+        start = pl.multiple_of((part % CUTS) * fine, fine)
+        return tgu.at[part // CUTS, turn, pl.ds(start, fine)]
+
+    def kind_of(part):
+        return 1 if isinstance(part, int) and part == DOWN else 0
 
     def pair_copy(kind, part):
-        send = pair_send.at[kind, part]
+        send = pair_send.at[kind_of(part)]
         if kind == 0:
-            return remote(thru_at(0, part), main_at(z, y, part, tp), send, main_recv.at[1, part], pair_dev)
+            return remote(thru_at(0, part), main_at(z, y, part, tp), send, main_recv.at[0, part], pair_dev)
         if kind == 1:
-            return remote(main_at(z, y, part, tp), thru_at(1, part), send, thru_recv.at[1, part], pair_dev)
+            return remote(main_at(z, y, part, tp), thru_at(1, part), send, thru_recv.at[0, part], pair_dev)
         return remote(
-            thru_at(kind, part), main_at(shard_z(kind), y, part, tp), send, main_recv.at[kind, part], pair_dev
+            thru_at(kind, part), main_at(shard_z(kind), y, part, tp), send, main_recv.at[kind - 1, part], pair_dev
         )
 
     def mid_copy(kind, part):
-        send = mid_send.at[kind, part]
+        send = mid_send.at[kind_of(part)]
         turn = 2 + kind // 2
         if kind % 2 == 0:
             ref = main_at(shard_z(kind // 2), y, part, tp)
-            return remote(ref, ref, send, main_recv.at[turn, part], mid_dev)
-        return remote(thru_at(kind // 2, part), thru_at(turn, part), send, thru_recv.at[turn, part], mid_dev)
+            return remote(ref, ref, send, main_recv.at[turn - 1, part], mid_dev)
+        return remote(thru_at(kind // 2, part), thru_at(turn, part), send, thru_recv.at[turn - 1, part], mid_dev)
 
     def main_in(turn, part):
         ref = main_at(shard_z(turn), y, part, tp)
-        return remote(ref, ref, pair_send.at[0, part], main_recv.at[turn, part], pair_dev)
+        return remote(ref, ref, pair_send.at[0], main_recv.at[turn - 1, part], pair_dev)
 
     def thru_in(turn, part):
         ref = thru_at(turn, part)
-        return remote(ref, ref, pair_send.at[0, part], thru_recv.at[turn, part], pair_dev)
+        return remote(ref, ref, pair_send.at[0], thru_recv.at[turn - 1, part], pair_dev)
 
     def y_copy(turn, part):
         ref = main_at(shard_z(turn), y, part, tp)
-        return remote(ref, ref, y_send.at[turn, part], y_recv.at[turn, part], y_dev)
+        return remote(ref, ref, y_send.at[kind_of(part)], y_recv.at[turn, part], y_dev)
 
     def y_in(turn, part):
         ref = main_at(shard_z(turn), 1 - y, part, tp)
-        return remote(ref, ref, y_send.at[turn, part], y_recv.at[turn, part], y_dev)
+        return remote(ref, ref, y_send.at[kind_of(part)], y_recv.at[turn, part], y_dev)
 
     def c_copy(turn, side, part):
         ref = main_at(shard_z(turn), y + side - 2 * side * y, part, tp)
-        return remote(ref, ref, c_send.at[turn, side, part], c_recv.at[turn, side, part], c_dev)
+        return remote(ref, ref, c_send.at[kind_of(part)], c_recv.at[turn, side, kind_of(part)], c_dev)
 
     def c_in(turn, side, part):
-        ref = main_at(shard_z(turn), y + side - 2 * side * y, part, 1 - tp)
-        return remote(ref, ref, c_send.at[turn, side, part], c_recv.at[turn, side, part], c_dev)
+        shard_y = y + side - 2 * side * y
+        if part == DOWN:
+            ref = main_at(shard_z(turn), shard_y, DOWN, 1 - tp)
+        else:
+            spare = pl.ds(pl.multiple_of((1 - tp) * units, 128), units)
+            start = pl.multiple_of(shard_y * depth, depth)
+            ref = wgu.at[:, shard_z(turn), pl.ds(start, depth), spare]
+        return remote(ref, ref, c_send.at[kind_of(part)], c_recv.at[turn, side, kind_of(part)], c_dev)
 
     def tok_pair(piece):
         part = pl.ds(piece * piece_tok, piece_tok)
         return remote(
-            rows.at[0, part], rows.at[1, part], tok_send.at[piece], tok_recv.at[piece], pair_dev
+            rows.at[0, part], rows.at[1, part], tok_send.at[0], tok_recv.at[piece], pair_dev
         )
 
     def tok_far(piece):
         return remote(
             rows.at[1, pl.ds(piece * piece_tok, piece_tok)],
             rows.at[1, pl.ds(n_tok + piece * piece_tok, piece_tok)],
-            tok_send.at[PIECES + piece], tok_recv.at[PIECES + piece], x_dev,
+            tok_send.at[1], tok_recv.at[PIECES + piece], x_dev,
         )
 
     def tok_x():
         return remote(
             rows.at[0, pl.ds(0, n_tok)], rows.at[0, pl.ds(n_tok, n_tok)],
-            tok_send.at[2 * PIECES], tok_recv.at[2 * PIECES], x_dev,
+            tok_send.at[2], tok_recv.at[2 * PIECES], x_dev,
         )
 
     def part_x(block, far):
         return remote(
-            staged.at[block, far, 1], landed_x.at[block, far], px_send.at[block, far], px_recv.at[block, far], x_dev
+            staged.at[block, far, 1], landed_x.at[block, far], px_send, px_recv.at[block, far], x_dev
         )
 
     def part_z(block):
-        return remote(summed.at[block], landed_z.at[block], pz_send.at[block], pz_recv.at[block], pair_dev)
+        return remote(summed.at[block], landed_z.at[block], pz_send, pz_recv.at[block], pair_dev)
 
     def early_z(block):
-        return remote(staged.at[block, 1, 0], landed_z.at[block], pz_send.at[block], pz_recv.at[block], pair_dev)
-
-    def place_of(turn):
-        late = turn // 2
-        return (1 - late) * (shard_z(turn) - 2 * side_z) + 2 * late
+        return remote(staged.at[block, 1, 0], landed_z.at[block], pz_send, pz_recv.at[block], pair_dev)
+
+    def place_of(turn, side):
+        return side * (shard_z(turn) - 2 * side_z) + (1 - side) * (2 + turn // 2)
 
     def early_far(block, place):
         return remote(
-            staged.at[block, 1, 1], landed_f.at[place], pf_send.at[place], pf_recv.at[place], pair_dev
+            staged.at[block, 1, 1], landed_f.at[place], pf_send, pf_recv.at[place], pair_dev
         )
 
     def scale_copy():
@@ -234,14 +243,14 @@
     base = rep * 2 * units
     both = pl.ds(pl.multiple_of(base, 128), 2 * units)
     loads = []
-    for part in range(4):
-        source = gate_ref if part // 2 == 0 else up_ref
-        span = pl.ds((part % 2) * half, half)
-        loads.append((source.at[span, both], raw_gu.at[part // 2, span]))
+    for part in range(DOWN):
+        source = gate_ref if part // CUTS == 0 else up_ref
+        span = pl.ds((part % CUTS) * fine, fine)
+        loads.append((source.at[span, both], raw_gu.at[part // CUTS, span]))
     loads.append((down_ref.at[both], raw_d))
     loads += [(tok_ref, tok), (gain_ref, gain), (gscale_ref, gscale), (uscale_ref, uscale), (dscale_ref, dscale)]
     loads = [pltpu.make_async_copy(*pair, load_sem.at[index]) for index, pair in enumerate(loads)]
-    for index in (0, 5, 6, 1, 2, 3, 4, 7, 8, 9):
+    for index in (0, 1, DOWN + 1, DOWN + 2, *range(2, DOWN + 1), DOWN + 3, DOWN + 4, DOWN + 5):
         loads[index].start()
 
     mine = pl.ds(pl.multiple_of(outer * units, 128), units)
@@ -250,10 +259,10 @@
 
     def round_part(part):
         loads[part].wait()
-        span = slice((part % 2) * half, (part % 2 + 1) * half)
-        start = pl.multiple_of(y * depth + (part % 2) * half, half)
-        wgu[part // 2, z, pl.ds(start, half), lanes] = raw_gu[part // 2, span, mine].astype(jnp.bfloat16)
-        tgu[part // 2, 0, span] = raw_gu[part // 2, span, theirs].astype(jnp.bfloat16)
+        span = slice((part % CUTS) * fine, (part % CUTS + 1) * fine)
+        start = pl.multiple_of(y * depth + (part % CUTS) * fine, fine)
+        wgu[part // CUTS, z, pl.ds(start, fine), lanes] = raw_gu[part // CUTS, span, mine].astype(jnp.bfloat16)
+        tgu[part // CUTS, 0, span] = raw_gu[part // CUTS, span, theirs].astype(jnp.bfloat16)
 
     def send_part(part):
         pair_copy(0, part).start()
@@ -268,13 +277,15 @@
     round_part(0)
     pl.semaphore_wait(barrier, 4 + inner)
     send_part(0)
-    loads[5].wait()
-    loads[6].wait()
+    round_part(1)
+    send_part(1)
+    loads[DOWN + 1].wait()
+    loads[DOWN + 2].wait()
     values = tok[...].astype(jnp.float32)
     inverse = lax.rsqrt(jnp.mean(values * values, axis=-1, keepdims=True) + EPS_VALUE)
     rows[0, :n_tok] = (values * inverse * gain[...]).astype(jnp.bfloat16)
     tok_x().start()
-    for part in range(1, 4):
+    for part in range(2, DOWN):
         round_part(part)
         send_part(part)
     for piece in range(PIECES):
@@ -282,15 +293,13 @@
 
     @pl.when(is_inner)
     def _():
-        for part in range(4):
-            mid_copy(1, part).start()
+        each(DOWN, lambda part: mid_copy(1, part).start())
 
     @pl.when(is_outer)
     def _():
-        for part in range(4):
-            pair_copy(1, part).start()
-
-    for index in (7, 8, 9):
+        each(DOWN, lambda part: pair_copy(1, part).start())
+
+    for index in (DOWN + 3, DOWN + 4, DOWN + 5):
         loads[index].wait()
     first_row = (base + outer * units) // 128
     for index in range(units // 128):
@@ -322,7 +331,8 @@
         tok_far(piece).start()
 
     def c_wait(turn):
-        each(8, lambda index: c_in(turn, index // 4, index % 4).wait_recv())
+        for side in range(2):
+            c_in(turn, side, 0).wait_recv()
 
     def term(far, matrix, turn):
         shard = shard_z(turn)
@@ -343,6 +353,19 @@
     def add_late(part):
         acc[part % 2, part // 2] += term(part // 2, part % 2, 2)
 
+    def half_term(far, matrix, span, side):
+        shard = shard_z(3)
+        shard_y = y + side - 2 * side * y
+        start = pl.multiple_of((shard * 2 + shard_y) * depth, depth)
+        inside = pl.multiple_of(shard_y * depth, depth)
+        return jnp.dot(
+            rows[far, span, pl.ds(start, depth)], wgu[matrix, shard, pl.ds(inside, depth)],
+            preferred_element_type=jnp.float32,
+        )
+
+    def add_last(part):
+        acc[part % 2, part // 2] += half_term(part // 2, part % 2, pl.ds(0, 2 * n_tok), 0)
+
     def first(part):
         take_main(1, part)
 
@@ -352,11 +375,11 @@
 
         take_y(0, part)
 
-    each(4, first)
+    each(DOWN, first)
 
     @pl.when(is_inner)
     def _():
-        each(4, lambda part: take_main(2, part))
+        each(DOWN, lambda part: take_main(2, part))
 
     @pl.when(is_outer)
     def _():
@@ -370,11 +393,11 @@
 
         take_y(1, part)
 
-        @pl.when((part == 1) | (part == 2))
-        def _():
-            take_rows(part - 1)
-
-    each(4, second)
+        @pl.when((part == 3) | (part == 5))
+        def _():
+            take_rows((part - 3) // 2)
+
+    each(DOWN, second)
     take_rows(2)
 
     def pass_outward(part):
@@ -387,15 +410,15 @@
             take_main(3, part)
             take_y(2, part)
 
-            @pl.when(part == 1)
+            @pl.when(part == 3)
             def _():
                 take_rows(3)
 
-            @pl.when(part == 2)
-            def _():
-                pass_outward(0)
-
-        each(4, third)
+            @pl.when(part > 5)
+            def _():
+                pass_outward(part - 6)
+
+        each(DOWN, third)
         y_copy(0, DOWN).start()
 
     @pl.when(is_outer)
@@ -409,55 +432,68 @@
     @pl.when(is_inner)
     def _():
         c_wait(2)
-
-        def fourth(part):
-            @pl.when(part < 3)
-            def _():
-                pass_outward(part + 1)
-
-            @pl.when(part == 2)
+        c_in(3, 0, 0).wait_recv()
+
+        def fourth(chunk):
+            @pl.when(chunk < 3)
+            def _():
+                for ahead in (2, 3):
+                    pass_outward(2 * chunk + ahead)
+
+            @pl.when(chunk == 2)
             def _():
                 mid_copy(1, DOWN).start()
                 mid_copy(0, DOWN).start()
 
-            add_early(part)
-            add_late(part)
-            thru_in(3, part).wait_recv()
-            pair_copy(3, part).start()
-            take_y(3, part)
+            add_early(chunk)
+            add_late(chunk)
+            for part in (2 * chunk, 2 * chunk + 1):
+                thru_in(3, part).wait_recv()
+                pair_copy(3, part).start()
+                take_y(3, part)
+            add_last(chunk)
 
         each(4, fourth)
         pair_copy(0, DOWN).start()
 
     @pl.when(is_outer)
     def _():
-        def fourth(part):
-            take_main(2, part)
-
-            @pl.when(part > 0)
-            def _():
-                take_y(2, part - 1)
-
-            add_early(part)
+        def fourth(chunk):
+            for part in (2 * chunk, 2 * chunk + 1):
+                take_main(2, part)
+
+                @pl.when(chunk > 0)
+                def _():
+                    take_y(2, part - 2)
+
+            add_early(chunk)
 
         each(4, fourth)
 
-        def fifth(part):
-            take_main(3, part)
-
-            @pl.when(part == 0)
-            def _():
-                take_y(2, 3)
+        def fifth(chunk):
+            for part in (2 * chunk, 2 * chunk + 1):
+                take_main(3, part)
+
+                @pl.when(chunk == 0)
+                def _():
+                    take_y(2, part + 6)
+
+                @pl.when(chunk > 0)
+                def _():
+                    take_y(3, part - 2)
+
+            @pl.when(chunk == 0)
+            def _():
                 c_wait(2)
 
-            @pl.when(part > 0)
-            def _():
-                take_y(3, part - 1)
-
-            add_late(part)
+            add_late(chunk)
 
         each(4, fifth)
-        take_y(3, 3)
+        c_in(3, 0, 0).wait_recv()
+        take_y(3, 6)
+        each(2, add_last)
+        take_y(3, 7)
+        each(2, lambda chunk: add_last(chunk + 2))
         take_y(0, DOWN)
         c_in(0, 1, DOWN).wait_recv()
 
@@ -465,14 +501,16 @@
         return shard_z(turn) * 2 + y + side - 2 * side * y
 
     def z_first(turn, side):
-        return ((side == 1) & (turn < 2)) | ((side == 0) & (turn == 2))
+        return ((turn < 2) & ((side == 1) | (turn + inner == 1))) | ((turn == 2) & (side == 0))
 
     def send_off(turn, side, far, near_x):
         block = block_of(turn, side)
         ahead = z_first(turn, side)
         crossing = far + inner == 1
 
-        @pl.when((near_x == 1) & (jnp.logical_not(ahead) | jnp.logical_not(crossing)))
+        held = is_outer & (turn == 2) & (side == 1) & (far == 0)
+
+        @pl.when((near_x == 1) & jnp.logical_not((ahead & crossing) | held))
         def _():
             part_x(block, far).start()
 
@@ -480,7 +518,7 @@
         def _():
             @pl.when(near_x == 1)
             def _():
-                early_far(block, place_of(turn)).start()
+                early_far(block, place_of(turn, side)).start()
 
             @pl.when(near_x == 0)
             def _():
@@ -490,7 +528,7 @@
         return dscale[:, pl.ds(pl.multiple_of(block * cols, cols), cols)]
 
     scale_in().wait_recv()
-    c_wait(3)
+    c_in(3, 1, 0).wait_recv()
     c_in(0, 0, DOWN).wait_recv()
 
     def activate(index):
@@ -498,11 +536,14 @@
         far = inner + swap - 2 * inner * swap
         near_x = 1 - index // 2
         span = pl.ds(pl.multiple_of(near_x * n_tok, n_tok), n_tok)
-        shard = shard_z(3)
-        depths = pl.ds(pl.multiple_of(shard * 2 * depth, 2 * depth), 2 * depth)
         pre = []
+
+        @pl.when(index == 1 + inner)
+        def _():
+            take_main(1, DOWN)
+
         for matrix in range(2):
-            last = jnp.dot(rows[far, span, depths], wgu[matrix, shard], preferred_element_type=jnp.float32)
+            last = half_term(far, matrix, span, 1)
             scale = jnp.concatenate(
                 [scales[0, matrix:matrix + 1], scales[1, matrix:matrix + 1]], axis=1
             )
@@ -544,7 +585,7 @@
 
     def late_x(turn, side):
         block = block_of(turn, side)
-        place = place_of(turn)
+        place = place_of(turn, side)
         early_far(block, place).wait_recv()
         total = staged[block, 0, 1].astype(jnp.float32) + landed_f[place].astype(jnp.float32)
         staged[block, 0, 1] = total.astype(jnp.bfloat16)
@@ -554,9 +595,13 @@
         step = index + 1
         swap = inner * (step // 3) * (1 - step // 4)
 
-        @pl.when(is_inner & (step == 4))
-        def _():
-            late_x(0, 1)
+        @pl.when(is_inner & (step == 2))
+        def _():
+            take_main(2, DOWN)
+
+        @pl.when(is_inner | (step > 1))
+        def _():
+            take_y(step - 1, DOWN)
 
         def sides(order):
             side = order + swap - 2 * order * swap
@@ -564,13 +609,9 @@
 
             @pl.when((turn < 4) & ((side == 0) | (turn > 0) | is_inner))
             def _():
-                @pl.when(side == 0)
+                @pl.when(is_inner & (side == 0) & (turn == 3))
                 def _():
-                    take_main(turn, DOWN)
-
-                @pl.when(side == 1)
-                def _():
-                    take_y(turn, DOWN)
+                    take_main(3, DOWN)
 
                 c_in(turn, side, DOWN).wait_recv()
                 produce(turn, side)
@@ -596,23 +637,40 @@
             def _():
                 late_x(1, 1)
 
+            @pl.when(step == 4)
+            def _():
+                late_x(0, 0)
+                late_x(0, 1)
+
+        @pl.when(is_outer & (step < 3))
+        def _():
+            take_main(step + 1, DOWN)
+
+        @pl.when(is_outer & (step == 4))
+        def _():
+            part_x(block_of(2, 1), 0).start()
+
         def folds(side):
-            @pl.when(step - 1 - side >= 0)
-            def _():
-                fold(step - 1 - side, side)
+            later = outer * (1 - side) * (1 - (step - 1) // 2)
+
+            @pl.when((step - 1 - side >= 0) & (is_inner | (side == 1) | (step > 1)))
+            def _():
+                fold(step - 1 - side - later, side)
 
         each(2, folds)
 
     each(4, down_step)
+
+
+    @pl.when(is_inner)
+    def _():
+        late_x(2, 0)
+
     fold(3, 1)
-
-    @pl.when(is_inner)
-    def _():
-        late_x(2, 0)
 
     def out_copy(block):
         span = pl.ds(pl.multiple_of(block * cols, cols), cols)
-        return pltpu.make_async_copy(result.at[:, span], out_ref.at[:, span], out_sem.at[block])
+        return pltpu.make_async_copy(result.at[:, span], out_ref.at[:, span], out_sem)
 
     def finish(index):
         block = block_of(outer * (index // 2) + inner * (3 - index // 2), index % 2)
@@ -625,58 +683,37 @@
 
     each(8, finish)
 
-    def drain_part(part):
-        pair_copy(0, part).wait_send()
-
-        @pl.when(is_outer)
-        def _():
-            pair_copy(1, part).wait_send()
-
-        @pl.when(is_inner)
-        def _():
-            pair_copy(2, part).wait_send()
-            pair_copy(3, part).wait_send()
-            for kind in range(4):
-                mid_copy(kind, part).wait_send()
-
-        def turns(turn):
-            y_copy(turn, part).wait_send()
-            c_copy(turn, 0, part).wait_send()
-            c_copy(turn, 1, part).wait_send()
-
-        each(4, turns)
-
-    each(4, drain_part)
-    drain_part(DOWN)
-
-    def drain_rows(piece):
-        tok_pair(piece).wait_send()
-        tok_far(piece).wait_send()
-
-    each(PIECES, drain_rows)
-    tok_x().wait_send()
+    def sent(src, send):
+        remote(src, src, send, pf_recv.at[0], c_dev).wait_send()
+
+    near = pl.ds(0, units)
+
+    def drain(turns, pair_turns):
+        for count, send in ((pair_turns, pair_send), (turns, mid_send)):
+            if count:
+                sent(wgu.at[:, pl.ds(0, count), pl.ds(0, depth), near], send.at[0])
+                sent(wd.at[pl.ds(0, count), near], send.at[1])
+
+    @pl.when(is_inner)
+    def _():
+        drain(4, 3)
+        sent(staged.at[pl.ds(0, 4)], px_send)
+
+    @pl.when(is_outer)
+    def _():
+        drain(0, 2)
+        sent(staged.at[pl.ds(0, 3)], px_send)
+        sent(landed_f, pf_send)
+
+    sent(wgu.at[:, :, pl.ds(0, depth), near], y_send.at[0])
+    sent(wd.at[pl.ds(0, 4), near], y_send.at[1])
+    sent(wgu.at[:, :, :, near], c_send.at[0])
+    sent(wd.at[:, near], c_send.at[1])
+    for index in range(3):
+        sent(rows.at[0, pl.ds(0, n_tok)], tok_send.at[index])
     scale_copy().wait_send()
-
-    def drain_block(turn):
-        def sides(side):
-            block = block_of(turn, side)
-            part_x(block, 0).wait_send()
-            part_z(block).wait_send()
-            ahead = z_first(turn, side)
-
-            @pl.when(is_inner | jnp.logical_not(ahead))
-            def _():
-                part_x(block, 1).wait_send()
-
-            @pl.when(is_outer & ahead)
-            def _():
-                early_far(block, place_of(turn)).wait_send()
-
-            out_copy(block).wait()
-
-        each(2, sides)
-
-    each(4, drain_block)
+    sent(landed_z, pz_send)
+    pltpu.make_async_copy(result, out_ref, out_sem).wait()
 
 
 def kernel_body(tokens, norm_gain, gate_weight, gate_scale, up_weight, up_scale, down_weight, down_scale, sizes):
@@ -689,7 +726,7 @@
     anywhere = pl.BlockSpec(memory_space=pl.ANY)
     bf, wide = jnp.bfloat16, jnp.float32
     dma = pltpu.SemaphoreType.DMA
-    turns, parts = 4, 5
+    turns, parts = 4, DOWN + 1
     return pl.pallas_call(
         ffn_kernel,
         out_shape=jax.ShapeDtypeStruct((n_tok, width), bf),
@@ -715,13 +752,13 @@
             pltpu.VMEM((n_fs, 2, n_tok, cols), bf),
             pltpu.VMEM((n_fs, n_tok, cols), bf),
             pltpu.VMEM((n_fs, n_tok, cols), bf),
-            pltpu.VMEM((3, n_tok, cols), bf),
+            pltpu.VMEM((4, n_tok, cols), bf),
             pltpu.VMEM((n_tok, width), bf),
-            dma((10,)), dma((n_fs,)), dma, dma,
-            dma((turns, parts)), dma((turns, parts)), dma((turns, parts)), dma((turns, parts)),
-            dma((turns, parts)), dma((turns, parts)), dma((turns, 2, parts)), dma((turns, 2, parts)),
-            dma((2 * PIECES + 1,)), dma((2 * PIECES + 1,)),
-            dma((n_fs, 2)), dma((n_fs, 2)), dma((n_fs,)), dma((n_fs,)), dma((3,)), dma((3,)),
+            dma((DOWN + 6,)), dma, dma, dma,
+            dma((2,)), dma((2,)), dma((turns - 1, parts)), dma((turns - 1, parts)),
+            dma((2,)), dma((turns, parts)), dma((2,)), dma((turns, 2, 2)),
+            dma((3,)), dma((2 * PIECES + 1,)),
+            dma, dma((n_fs, 2)), dma, dma((n_fs,)), dma, dma((4,)),
         ],
         compiler_params=pltpu.CompilerParams(
             collective_id=0, has_side_effects=True, vmem_limit_bytes=62 * 1024 * 1024
@@ -736,6 +773,7 @@
     n_rep, n_fs, n_tp = (mesh.shape[name] for name in ("rep", "fs", "tp"))
     units = gate_weight.shape[1] // (n_tp * n_rep * 2)
     aligned = units % 128 == 0 and down_weight.shape[1] // n_fs % 128 == 0
+    aligned = aligned and gate_weight.shape[0] // n_fs % (32 * CUTS) == 0
     return aligned and n_rep == 2 and n_fs == 8 and n_tp == 2
 
 

time: 126 us -> 122 us (0.968); the launches traced: 126 us -> 121 us
  Pallas kernels: 124 us -> 118 us
    pallas_call x1, Pallas kernels: 124 us -> 118 us  [kernel_body(): pl.pallas_call(ffn_kernel, out_shape=jax.ShapeDtypeStruct((n_tok, width),...]
where the time goes in v3:
time: 122 us; the launch traced here: 121 us
  Pallas kernels  118 us (97%)
  local copies, waits for them, and re-layouts  2.3 us (2%)
    pallas_call x1, Pallas kernels, kernel_body(): pl.pallas_call(ffn_kernel, out_shape=jax.ShapeDtypeStruct((n_tok, width),...  118 us

profile of v3, /device:TPU:17, one launch (start us, length us, event | category | flops | bytes accessed | tf_op | source)
XLA Modules:
  0.0 120.7 jit_solution(11573151035854303922)
XLA Ops:
  0.0 118.4 %shard_map.82 = bf16[256,2048]{1,0:T(8,128)(2,1)} custom-call(bf16[256,2048]{1,0:T(8,128)(2,1)} %tok_ref.1, f32[1,2048]{1,0:T(1,128)} %bitcast.6, f32[256,2560]{1,0:T(8,128)} %gate_ref.1, f32[20,128]{1,0:T(8,128)} %bitcast.4, f32[256,2560]{1,0:T(8,128)} %up_ref.1, f32[20,128]{1,0:T(8,128)} %bitcast.5, f32[2560,256]{1,0:T(8,128)} %down_ref.1, f32[1,2048]{1,0:T(1,128)} %bitcast.7), custom_call_target="tpu_custom_call" | custom-call | tf_op jit(solution)/shard_map/pallas_call | solution.py:730
  118.4 2.3 %copy.10 = bf16[256,2048]{1,0:T(8,128)(2,1)} copy(bf16[256,2048]{1,0:T(8,128)(2,1)} %shard_map.82) | data formatting | bytes 2097152

commit v4 on v0

v4 whole, which is shorter than its diff:
```python
import functools

import jax
import jax.numpy as jnp
from jax import lax
from jax.experimental import pallas as pl
from jax.experimental.pallas import tpu as pltpu
from jax.sharding import PartitionSpec as P

EPS_VALUE = 1e-06


def from_partner(shard, axis, distance):
    return lax.ppermute(shard, axis, [(i, i ^ 1 << distance) for i in range(lax.axis_size(axis))])


def normalize(token_rows, norm_gain):
    values = token_rows.astype(jnp.float32)
    inverse = lax.rsqrt(jnp.mean(values * values, axis=-1, keepdims=True) + EPS_VALUE)
    return (values * inverse * norm_gain).astype(jnp.bfloat16)


def body(tokens, norm_gain, gate_weight, gate_scale, up_weight, up_scale, down_weight, down_scale):
    normed = normalize(tokens, norm_gain)
    gate_bf = gate_weight.astype(jnp.bfloat16)
    up_bf = up_weight.astype(jnp.bfloat16)
    down_bf = down_weight.astype(jnp.bfloat16)
    rep_index = lax.axis_index("rep")
    half_cols = gate_bf.shape[1] // 2
    half_rows = down_bf.shape[0] // 2
    own_gate = lax.dynamic_slice_in_dim(gate_bf, rep_index * half_cols, half_cols, 1)
    own_up = lax.dynamic_slice_in_dim(up_bf, rep_index * half_cols, half_cols, 1)
    own_down = lax.dynamic_slice_in_dim(down_bf, rep_index * half_rows, half_rows, 0)
    own_parts = (
        lax.all_gather(own_gate, "fs", axis=0, tiled=True),
        lax.all_gather(own_up, "fs", axis=0, tiled=True),
        lax.all_gather(own_down, "fs", axis=1, tiled=True),
    )
    far_parts = from_partner((own_parts[0], own_parts[1], own_parts[2]), "rep", 0)
    is_first = rep_index == 0

    def joined(own_part, far_part, axis_dim):
        return jnp.where(
            is_first,
            jnp.concatenate([own_part, far_part], axis_dim),
            jnp.concatenate([far_part, own_part], axis_dim),
        )

    gate_full = joined(own_parts[0], far_parts[0], 1)
    up_full = joined(own_parts[1], far_parts[1], 1)
    down_full = joined(own_parts[2], far_parts[2], 0)
    slab_rows = lax.all_gather(normed, "tp", axis=0, tiled=True)
    gate_pre = jnp.dot(slab_rows, gate_full, preferred_element_type=jnp.float32) * gate_scale
    up_pre = jnp.dot(slab_rows, up_full, preferred_element_type=jnp.float32) * up_scale
    hidden = (jax.nn.silu(gate_pre) * up_pre).astype(jnp.bfloat16)
    partial_value = (
        jnp.dot(hidden, down_full, preferred_element_type=jnp.float32) * down_scale
    ).astype(jnp.bfloat16)
    partial_value = lax.optimization_barrier(partial_value)
    return lax.psum_scatter(
        partial_value.astype(jnp.float32).astype(jnp.bfloat16),
        "tp",
        scatter_dimension=0,
        tiled=True,
    )


MESH = pl.DeviceIdType.MESH
CUTS = 4
DOWN = 2 * CUTS
PIECES = 4


def each(count, step):
    def go(index, carry):
        step(index)
        return carry

    lax.fori_loop(0, count, go, 0)


def ffn_kernel(
    tok_ref, gain_ref, gate_ref, gscale_ref, up_ref, uscale_ref, down_ref, dscale_ref, out_ref,
    tok, gain, gscale, uscale, dscale, raw_gu, raw_d, wgu, wd, tgu, td, scales, rows, acc, hid,
    staged, landed_x, summed, landed_z, landed_f, result,
    out_sem, px_send, px_recv, pz_send, pz_recv, pf_send,
):
    n_tok = tok.shape[0]
    piece_tok = n_tok // PIECES
    units = tgu.shape[3]
    depth = tgu.shape[2]
    fine = depth // CUTS
    cols = wd.shape[2]

    rep = lax.axis_index("rep")
    fs = lax.axis_index("fs")
    tp = lax.axis_index("tp")
    z = fs // 2
    y = fs % 2
    side_z = z // 2
    inner = (z + side_z) % 2
    outer = 1 - inner
    is_inner = inner == 1
    is_outer = inner == 0
    z_pair = 1 + 4 * side_z - z

    pair_dev = (rep, z_pair * 2 + y, tp)
    mid_dev = (rep, (3 - z) * 2 + y, tp)
    y_dev = (rep, z * 2 + 1 - y, tp)
    x_dev = (1 - rep, fs, tp)
    c_dev = (rep, fs, 1 - tp)

    def remote(src, dst, send, recv, device):
        return pltpu.make_async_remote_copy(
            src_ref=src, dst_ref=dst, send_sem=send, recv_sem=recv, device_id=device, device_id_type=MESH
        )

    def shard_z(turn):
        if isinstance(turn, int):
            return (z, z_pair, 2 - side_z, 3 - 3 * side_z)[turn]
        late = turn // 2
        odd = turn % 2
        early = (1 - odd) * z + odd * z_pair
        return (1 - late) * early + late * ((1 - odd) * (2 - side_z) + odd * (3 - 3 * side_z))

    def part_x(block, far):
        return remote(
            staged.at[block, far, 1], landed_x.at[block, far], px_send, px_recv.at[block, far], x_dev
        )

    def part_z(block):
        return remote(summed.at[block], landed_z.at[block], pz_send, pz_recv.at[block], pair_dev)

    def block_of(turn, side):
        return shard_z(turn) * 2 + y + side - 2 * side * y

    def z_first(turn, side):
        return ((turn < 2) & ((side == 1) | (turn + inner == 1))) | ((turn == 2) & (side == 0))

    def fold(turn, side):
        block = block_of(turn, side)

        @pl.when(is_inner | jnp.logical_not(z_first(turn, side)))
        def _():
            part_x(block, 1).wait_recv()
            total = staged[block, 1, 0].astype(jnp.float32) + landed_x[block, 1].astype(jnp.float32)
            summed[block] = total.astype(jnp.bfloat16)
            part_z(block).start()

    def out_copy(block):
        span = pl.ds(pl.multiple_of(block * cols, cols), cols)
        return pltpu.make_async_copy(result.at[:, span], out_ref.at[:, span], out_sem)

    def sent(src, send):
        remote(src, src, send, px_recv.at[0, 0], c_dev).wait_send()

    near = pl.ds(0, units)

    def phases(
        load_sem, scale_send, scale_recv, pair_send, mid_send, main_recv, thru_recv, y_send, y_recv, c_send, c_recv,
        tok_send, tok_recv, pf_recv,
    ):
        barrier = pltpu.get_barrier_semaphore()
        for device in (pair_dev, y_dev, x_dev, c_dev):
            pl.semaphore_signal(barrier, inc=1, device_id=device, device_id_type=MESH)

        @pl.when(is_inner)
        def _():
            pl.semaphore_signal(barrier, inc=1, device_id=mid_dev, device_id_type=MESH)

        def main_at(shard, shard_y, part, core):
            lanes = pl.ds(pl.multiple_of(core * units, 128), units)
            if isinstance(part, int) and part == DOWN:
                return wd.at[shard * 2 + shard_y, lanes]
            start = pl.multiple_of(shard_y * depth + (part % CUTS) * fine, fine)
            return wgu.at[part // CUTS, shard, pl.ds(start, fine), lanes]

        def thru_at(turn, part):
            if isinstance(part, int) and part == DOWN:
                return td.at[turn]
            start = pl.multiple_of((part % CUTS) * fine, fine)
            return tgu.at[part // CUTS, turn, pl.ds(start, fine)]

        def kind_of(part):
            return 1 if isinstance(part, int) and part == DOWN else 0

        def pair_copy(kind, part):
            send = pair_send.at[kind_of(part)]
            if kind == 0:
                return remote(thru_at(0, part), main_at(z, y, part, tp), send, main_recv.at[0, part], pair_dev)
            if kind == 1:
                return remote(main_at(z, y, part, tp), thru_at(1, part), send, thru_recv.at[0, part], pair_dev)
            return remote(
                thru_at(kind, part), main_at(shard_z(kind), y, part, tp), send, main_recv.at[kind - 1, part], pair_dev
            )

        def mid_copy(kind, part):
            send = mid_send.at[kind_of(part)]
            turn = 2 + kind // 2
            if kind % 2 == 0:
                ref = main_at(shard_z(kind // 2), y, part, tp)
                return remote(ref, ref, send, main_recv.at[turn - 1, part], mid_dev)
            return remote(thru_at(kind // 2, part), thru_at(turn, part), send, thru_recv.at[turn - 1, part], mid_dev)

        def main_in(turn, part):
            ref = main_at(shard_z(turn), y, part, tp)
            return remote(ref, ref, pair_send.at[0], main_recv.at[turn - 1, part], pair_dev)

        def thru_in(turn, part):
            ref = thru_at(turn, part)
            return remote(ref, ref, pair_send.at[0], thru_recv.at[turn - 1, part], pair_dev)

        def y_copy(turn, part):
            ref = main_at(shard_z(turn), y, part, tp)
            return remote(ref, ref, y_send.at[kind_of(part)], y_recv.at[turn, part], y_dev)

        def y_in(turn, part):
            ref = main_at(shard_z(turn), 1 - y, part, tp)
            return remote(ref, ref, y_send.at[kind_of(part)], y_recv.at[turn, part], y_dev)

        def c_copy(turn, side, part):
            ref = main_at(shard_z(turn), y + side - 2 * side * y, part, tp)
            return remote(ref, ref, c_send.at[kind_of(part)], c_recv.at[turn, side, kind_of(part)], c_dev)

        def c_in(turn, side, part):
            shard_y = y + side - 2 * side * y
            if part == DOWN:
                ref = main_at(shard_z(turn), shard_y, DOWN, 1 - tp)
            else:
                spare = pl.ds(pl.multiple_of((1 - tp) * units, 128), units)
                start = pl.multiple_of(shard_y * depth, depth)
                ref = wgu.at[:, shard_z(turn), pl.ds(start, depth), spare]
            return remote(ref, ref, c_send.at[kind_of(part)], c_recv.at[turn, side, kind_of(part)], c_dev)

        def tok_pair(piece):
            part = pl.ds(piece * piece_tok, piece_tok)
            return remote(
                rows.at[0, part], rows.at[1, part], tok_send.at[0], tok_recv.at[piece], pair_dev
            )

        def tok_far(piece):
            return remote(
                rows.at[1, pl.ds(piece * piece_tok, piece_tok)],
                rows.at[1, pl.ds(n_tok + piece * piece_tok, piece_tok)],
                tok_send.at[1], tok_recv.at[PIECES + piece], x_dev,
            )

        def tok_x():
            return remote(
                rows.at[0, pl.ds(0, n_tok)], rows.at[0, pl.ds(n_tok, n_tok)],
                tok_send.at[2], tok_recv.at[2 * PIECES], x_dev,
            )

        def early_z(block):
            return remote(staged.at[block, 1, 0], landed_z.at[block], pz_send, pz_recv.at[block], pair_dev)

        def place_of(turn, side):
            return side * (shard_z(turn) - 2 * side_z) + (1 - side) * (2 + turn // 2)

        def early_far(block, place):
            return remote(
                staged.at[block, 1, 1], landed_f.at[place], pf_send, pf_recv.at[place], pair_dev
            )

        def scale_copy():
            return remote(scales.at[tp], scales.at[tp], scale_send, scale_recv, c_dev)

        def scale_in():
            return remote(scales.at[1 - tp], scales.at[1 - tp], scale_send, scale_recv, c_dev)

        base = rep * 2 * units
        both = pl.ds(pl.multiple_of(base, 128), 2 * units)
        loads = []
        for part in range(DOWN):
            source = gate_ref if part // CUTS == 0 else up_ref
            span = pl.ds((part % CUTS) * fine, fine)
            loads.append((source.at[span, both], raw_gu.at[part // CUTS, span]))
        loads.append((down_ref.at[both], raw_d))
        loads += [(tok_ref, tok), (gain_ref, gain), (gscale_ref, gscale), (uscale_ref, uscale), (dscale_ref, dscale)]
        loads = [pltpu.make_async_copy(*pair, load_sem.at[index]) for index, pair in enumerate(loads)]
        for index in (0, 1, DOWN + 1, DOWN + 2, *range(2, DOWN + 1), DOWN + 3, DOWN + 4, DOWN + 5):
            loads[index].start()

        mine = pl.ds(pl.multiple_of(outer * units, 128), units)
        theirs = pl.ds(pl.multiple_of(inner * units, 128), units)
        lanes = pl.ds(pl.multiple_of(tp * units, 128), units)

        def round_part(part):
            loads[part].wait()
            span = slice((part % CUTS) * fine, (part % CUTS + 1) * fine)
            start = pl.multiple_of(y * depth + (part % CUTS) * fine, fine)
            wgu[part // CUTS, z, pl.ds(start, fine), lanes] = raw_gu[part // CUTS, span, mine].astype(jnp.bfloat16)
            tgu[part // CUTS, 0, span] = raw_gu[part // CUTS, span, theirs].astype(jnp.bfloat16)

        def send_part(part):
            pair_copy(0, part).start()
            y_copy(0, part).start()

            @pl.when(is_inner)
            def _():
                mid_copy(0, part).start()

            c_copy(0, 0, part).start()

        round_part(0)
        pl.semaphore_wait(barrier, 4 + inner)
        send_part(0)
        round_part(1)
        send_part(1)
        loads[DOWN + 1].wait()
        loads[DOWN + 2].wait()
        values = tok[...].astype(jnp.float32)
        inverse = lax.rsqrt(jnp.mean(values * values, axis=-1, keepdims=True) + EPS_VALUE)
        rows[0, :n_tok] = (values * inverse * gain[...]).astype(jnp.bfloat16)
        tok_x().start()
        for part in range(2, DOWN):
            round_part(part)
            send_part(part)
        for piece in range(PIECES):
            tok_pair(piece).start()

        @pl.when(is_inner)
        def _():
            each(DOWN, lambda part: mid_copy(1, part).start())

        @pl.when(is_outer)
        def _():
            each(DOWN, lambda part: pair_copy(1, part).start())

        for index in (DOWN + 3, DOWN + 4, DOWN + 5):
            loads[index].wait()
        first_row = (base + outer * units) // 128
        for index in range(units // 128):
            span = slice(index * 128, (index + 1) * 128)
            scales[tp, 0:1, span] = gscale[pl.ds(first_row + index, 1), :]
            scales[tp, 1:2, span] = uscale[pl.ds(first_row + index, 1), :]
        scale_copy().start()
        loads[DOWN].wait()
        wd[fs, lanes] = raw_d[mine].astype(jnp.bfloat16)
        td[0] = raw_d[theirs].astype(jnp.bfloat16)
        c_copy(0, 0, DOWN).start()

        @pl.when(is_outer)
        def _():
            pair_copy(0, DOWN).start()
            pair_copy(1, DOWN).start()

        def take_main(turn, part):
            main_in(turn, part).wait_recv()
            y_copy(turn, part).start()
            c_copy(turn, 0, part).start()

        def take_y(turn, part):
            y_in(turn, part).wait_recv()
            c_copy(turn, 1, part).start()

        def take_rows(piece):
            tok_pair(piece).wait_recv()
            tok_far(piece).start()

        def c_wait(turn):
            for side in range(2):
                c_in(turn, side, 0).wait_recv()

        def term(far, matrix, turn):
            shard = shard_z(turn)
            span = pl.ds(pl.multiple_of(shard * 2 * depth, 2 * depth), 2 * depth)
            return jnp.dot(rows[far, :, span], wgu[matrix, shard], preferred_element_type=jnp.float32)

        def add_early(part):
            far, matrix = part // 2, part % 2

            @pl.when(part == 2)
            def _():
                for piece in range(PIECES):
                    tok_far(piece).wait_recv()

            acc[matrix, far] = term(far, matrix, 0)
            acc[matrix, far] += term(far, matrix, 1)

        def add_late(part):
            acc[part % 2, part // 2] += term(part // 2, part % 2, 2)

        def half_term(far, matrix, span, side):
            shard = shard_z(3)
            shard_y = y + side - 2 * side * y
            start = pl.multiple_of((shard * 2 + shard_y) * depth, depth)
            inside = pl.multiple_of(shard_y * depth, depth)
            return jnp.dot(
                rows[far, span, pl.ds(start, depth)], wgu[matrix, shard, pl.ds(inside, depth)],
                preferred_element_type=jnp.float32,
            )

        def add_last(part):
            acc[part % 2, part // 2] += half_term(part // 2, part % 2, pl.ds(0, 2 * n_tok), 0)

        def first(part):
            take_main(1, part)

            @pl.when(is_inner)
            def _():
                mid_copy(2, part).start()

            take_y(0, part)

        each(DOWN, first)

        @pl.when(is_inner)
        def _():
            each(DOWN, lambda part: take_main(2, part))

        @pl.when(is_outer)
        def _():
            y_copy(0, DOWN).start()

        def second(part):
            @pl.when(is_inner)
            def _():
                thru_in(2, part).wait_recv()
                pair_copy(2, part).start()

            take_y(1, part)

            @pl.when((part == 3) | (part == 5))
            def _():
                take_rows((part - 3) // 2)

        each(DOWN, second)
        take_rows(2)

        def pass_outward(part):
            thru_in(1, part).wait_recv()
            mid_copy(3, part).start()

        @pl.when(is_inner)
        def _():
            def third(part):
                take_main(3, part)
                take_y(2, part)

                @pl.when(part == 3)
                def _():
                    take_rows(3)

                @pl.when(part > 5)
                def _():
                    pass_outward(part - 6)

            each(DOWN, third)
            y_copy(0, DOWN).start()

        @pl.when(is_outer)
        def _():
            take_rows(3)

        tok_x().wait_recv()
        c_wait(0)
        c_wait(1)

        @pl.when(is_inner)
        def _():
            c_wait(2)
            c_in(3, 0, 0).wait_recv()

            def fourth(chunk):
                @pl.when(chunk < 3)
                def _():
                    for ahead in (2, 3):
                        pass_outward(2 * chunk + ahead)

                @pl.when(chunk == 2)
                def _():
                    mid_copy(1, DOWN).start()
                    mid_copy(0, DOWN).start()

                add_early(chunk)
                add_late(chunk)
                for part in (2 * chunk, 2 * chunk + 1):
                    thru_in(3, part).wait_recv()
                    pair_copy(3, part).start()
                    take_y(3, part)
                add_last(chunk)

            each(4, fourth)
            pair_copy(0, DOWN).start()

        @pl.when(is_outer)
        def _():
            def fourth(chunk):
                for part in (2 * chunk, 2 * chunk + 1):
                    take_main(2, part)

                    @pl.when(chunk > 0)
                    def _():
                        take_y(2, part - 2)

                add_early(chunk)

            each(4, fourth)

            def fifth(chunk):
                for part in (2 * chunk, 2 * chunk + 1):
                    take_main(3, part)

                    @pl.when(chunk == 0)
                    def _():
                        take_y(2, part + 6)

                    @pl.when(chunk > 0)
                    def _():
                        take_y(3, part - 2)

                @pl.when(chunk == 0)
                def _():
                    c_wait(2)

                add_late(chunk)

            each(4, fifth)
            c_in(3, 0, 0).wait_recv()
            take_y(3, 6)
            each(2, add_last)
            take_y(3, 7)
            each(2, lambda chunk: add_last(chunk + 2))
            take_y(0, DOWN)
            c_in(0, 1, DOWN).wait_recv()

        def send_off(turn, side, far, near_x):
            block = block_of(turn, side)
            ahead = z_first(turn, side)
            crossing = far + inner == 1

            held = is_outer & (turn == 2) & (side == 1) & (far == 0)

            @pl.when((near_x == 1) & jnp.logical_not((ahead & crossing) | held))
            def _():
                part_x(block, far).start()

            @pl.when(ahead & crossing & is_outer)
            def _():
                @pl.when(near_x == 1)
                def _():
                    early_far(block, place_of(turn, side)).start()

                @pl.when(near_x == 0)
                def _():
                    early_z(block).start()

        def scale_of(block):
            return dscale[:, pl.ds(pl.multiple_of(block * cols, cols), cols)]

        scale_in().wait_recv()
        c_in(3, 1, 0).wait_recv()
        c_in(0, 0, DOWN).wait_recv()

        def activate(index):
            far = 1 - index % 2
            near_x = 1 - index // 2
            span = pl.ds(pl.multiple_of(near_x * n_tok, n_tok), n_tok)
            pre = []

            @pl.when(index == 1 + inner)
            def _():
                take_main(1, DOWN)

            for matrix in range(2):
                last = half_term(far, matrix, span, 1)
                scale = jnp.concatenate(
                    [scales[0, matrix:matrix + 1], scales[1, matrix:matrix + 1]], axis=1
                )
                pre.append((acc[matrix, far, span] + last) * scale)
            hid[far, span] = (jax.nn.silu(pre[0]) * pre[1]).astype(jnp.bfloat16)

            def one(side, carry):
                block = block_of(0, side)
                product = jnp.dot(hid[far, span], wd[block], preferred_element_type=jnp.float32) * scale_of(block)
                staged[block, far, near_x] = product.astype(jnp.bfloat16)
                send_off(0, side, far, near_x)
                return carry

            lax.fori_loop(0, 1 + outer, one, 0)

        each(4, activate)

        def produce(turn, side):
            block = block_of(turn, side)

            def tile(index):
                far = 1 - index
                product = jnp.dot(hid[far], wd[block], preferred_element_type=jnp.float32) * scale_of(block)
                staged[block, far] = product.astype(jnp.bfloat16).reshape(2, n_tok, cols)
                for near_x in (1, 0):
                    send_off(turn, side, far, near_x)

            each(2, tile)

        def late_x(turn, side):
            block = block_of(turn, side)
            place = place_of(turn, side)
            early_far(block, place).wait_recv()
            total = staged[block, 0, 1].astype(jnp.float32) + landed_f[place].astype(jnp.float32)
            staged[block, 0, 1] = total.astype(jnp.bfloat16)
            part_x(block, 0).start()

        def down_step(index):
            step = index + 1
            swap = inner * (step // 3) * (1 - step // 4)

            @pl.when(is_inner & (step == 2))
            def _():
                take_main(2, DOWN)

            @pl.when(is_inner & (step == 4))
            def _():
                late_x(0, 0)

            @pl.when(is_inner | (step > 1))
            def _():
                take_y(step - 1, DOWN)

            def sides(order):
                side = order + swap - 2 * order * swap
                turn = step - side

                @pl.when((turn < 4) & ((side == 0) | (turn > 0) | is_inner))
                def _():
                    @pl.when(is_inner & (side == 0) & (turn == 3))
                    def _():
                        late_x(1, 1)
                        take_main(3, DOWN)

                    c_in(turn, side, DOWN).wait_recv()
                    produce(turn, side)

            each(2, sides)

            @pl.when(is_inner)
            def _():
                @pl.when(step == 1)
                def _():
                    thru_in(2, DOWN).wait_recv()
                    pair_copy(2, DOWN).start()
                    thru_in(1, DOWN).wait_recv()
                    mid_copy(3, DOWN).start()
                    mid_copy(2, DOWN).start()

                @pl.when(step == 2)
                def _():
                    thru_in(3, DOWN).wait_recv()
                    pair_copy(3, DOWN).start()

                @pl.when(step == 4)
                def _():
                    late_x(0, 1)

            @pl.when(is_outer & (step < 3))
            def _():
                take_main(step + 1, DOWN)

            @pl.when(is_outer & (step == 4))
            def _():
                part_x(block_of(2, 1), 0).start()

            def folds(side):
                @pl.when(step - 1 - side >= 0)
                def _():
                    fold(step - 1 - side, side)

            each(2, folds)

        each(4, down_step)


        @pl.when(is_inner)
        def _():
            late_x(2, 0)

        def drain(turns, pair_turns):
            for count, send in ((pair_turns, pair_send), (turns, mid_send)):
                if count:
                    sent(wgu.at[:, pl.ds(0, count), pl.ds(0, depth), near], send.at[0])
                    sent(wd.at[pl.ds(0, count), near], send.at[1])

        @pl.when(is_inner)
        def _():
            drain(4, 3)

        @pl.when(is_outer)
        def _():
            drain(0, 2)

        sent(wgu.at[:, :, pl.ds(0, depth), near], y_send.at[0])
        sent(wd.at[pl.ds(0, 4), near], y_send.at[1])
        sent(wgu.at[:, :, :, near], c_send.at[0])
        sent(wd.at[:, near], c_send.at[1])
        for index in range(3):
            sent(rows.at[0, pl.ds(0, n_tok)], tok_send.at[index])
        scale_copy().wait_send()

    dma = pltpu.SemaphoreType.DMA
    turns, parts = 4, DOWN + 1
    pl.run_scoped(
        phases,
        dma((DOWN + 6,)), dma, dma, dma((2,)), dma((2,)), dma((turns - 1, parts)), dma((turns - 1, parts)),
        dma((2,)), dma((turns, parts)), dma((2,)), dma((turns, 2, 2)), dma((3,)), dma((2 * PIECES + 1,)),
        dma((4,)),
    )
    fold(3, 1)

    def finish(index):
        block = block_of(outer * (index // 2) + inner * (3 - index // 2), index % 2)
        part_x(block, 0).wait_recv()
        part_z(block).wait_recv()
        total = staged[block, 0, 0].astype(jnp.float32) + landed_x[block, 0].astype(jnp.float32)
        total = total + landed_z[block].astype(jnp.float32)
        result[:, pl.ds(pl.multiple_of(block * cols, cols), cols)] = total.astype(result.dtype)
        out_copy(block).start()

    each(8, finish)

    sent(landed_z, pz_send)

    @pl.when(is_inner)
    def _():
        sent(staged.at[pl.ds(0, 4)], px_send)

    @pl.when(is_outer)
    def _():
        sent(staged.at[pl.ds(0, 3)], px_send)
        sent(staged.at[0], pf_send)

    pltpu.make_async_copy(result, out_ref, out_sem).wait()


def kernel_body(tokens, norm_gain, gate_weight, gate_scale, up_weight, up_scale, down_weight, down_scale, sizes):
    n_fs = sizes[1]
    n_tok, width = tokens.shape
    depth = gate_weight.shape[0]
    all_units = gate_weight.shape[1]
    units = all_units // (2 * sizes[0])
    cols = down_weight.shape[1]
    anywhere = pl.BlockSpec(memory_space=pl.ANY)
    bf, wide = jnp.bfloat16, jnp.float32
    dma = pltpu.SemaphoreType.DMA
    turns = 4
    return pl.pallas_call(
        ffn_kernel,
        out_shape=jax.ShapeDtypeStruct((n_tok, width), bf),
        in_specs=[anywhere] * 8,
        out_specs=anywhere,
        scratch_shapes=[
            pltpu.VMEM((n_tok, width), bf),
            pltpu.VMEM((1, width), wide),
            pltpu.VMEM((all_units // 128, 128), wide),
            pltpu.VMEM((all_units // 128, 128), wide),
            pltpu.VMEM((1, width), wide),
            pltpu.VMEM((2, depth, 2 * units), wide),
            pltpu.VMEM((2 * units, cols), wide),
            pltpu.VMEM((2, n_fs // 2, 2 * depth, 2 * units), bf),
            pltpu.VMEM((n_fs, 2 * units, cols), bf),
            pltpu.VMEM((2, turns, depth, units), bf),
            pltpu.VMEM((turns, units, cols), bf),
            pltpu.VMEM((2, 2, units), wide),
            pltpu.VMEM((2, 2 * n_tok, width), bf),
            pltpu.VMEM((2, 2, 2 * n_tok, 2 * units), wide),
            pltpu.VMEM((2, 2 * n_tok, 2 * units), bf),
            pltpu.VMEM((n_fs, 2, 2, n_tok, cols), bf),
            pltpu.VMEM((n_fs, 2, n_tok, cols), bf),
            pltpu.VMEM((n_fs, n_tok, cols), bf),
            pltpu.VMEM((n_fs, n_tok, cols), bf),
            pltpu.VMEM((4, n_tok, cols), bf),
            pltpu.VMEM((n_tok, width), bf),
            dma, dma, dma((n_fs, 2)), dma, dma((n_fs,)), dma,
        ],
        compiler_params=pltpu.CompilerParams(
            collective_id=0, has_side_effects=True, vmem_limit_bytes=62 * 1024 * 1024
        ),
    )(
        tokens, norm_gain[None, :], gate_weight, gate_scale.reshape(-1, 128), up_weight, up_scale.reshape(-1, 128),
        down_weight, down_scale[None, :],
    )


def fits_kernel(mesh, tokens, gate_weight, down_weight):
    n_rep, n_fs, n_tp = (mesh.shape[name] for name in ("rep", "fs", "tp"))
    units = gate_weight.shape[1] // (n_tp * n_rep * 2)
    aligned = units % 128 == 0 and down_weight.shape[1] // n_fs % 128 == 0
    aligned = aligned and gate_weight.shape[0] // n_fs % (32 * CUTS) == 0
    return aligned and n_rep == 2 and n_fs == 8 and n_tp == 2


def solution(mesh):
    sizes = tuple(mesh.shape[name] for name in ("rep", "fs", "tp"))

    def run(tokens, norm_gain, gate_weight, gate_scale, up_weight, up_scale, down_weight, down_scale):
        chosen = body
        if fits_kernel(mesh, tokens, gate_weight, down_weight):
            chosen = functools.partial(kernel_body, sizes=sizes)
        return jax.shard_map(
            chosen,
            mesh=mesh,
            in_specs=(
                P(("rep", "fs", "tp"), None),
                P(),
                P("fs", "tp"),
                P("tp"),
                P("fs", "tp"),
                P("tp"),
                P("tp", "fs"),
                P(),
            ),
            out_specs=P(("rep", "fs", "tp"), None),
            check_vma=False,
        )(tokens, norm_gain, gate_weight, gate_scale, up_weight, up_scale, down_weight, down_scale)

    return run
```

time: 175 us -> 119 us (0.68)
  Pallas kernels: 170 us -> 117 us
  local copies, waits for them, and re-layouts: 4.92 us -> 2.3 us
    pallas_call x1, Pallas kernels: 170 us -> 117 us  [kernel_body(): pl.pallas_call(ffn_kernel, out_shape=jax.ShapeDtypeStruct((n_tok, width),...]
    broadcast_in_dim x2 -> x0, local copies, waits for them, and re-layouts: 2.62 us -> none  [the longest x1 1.31 us: kernel_body(): gate_scale[None, :]]
where the time goes in v4:
time: 119 us
  Pallas kernels  117 us (98%)
  local copies, waits for them, and re-layouts  2.3 us (2%)
    pallas_call x1, Pallas kernels, kernel_body(): pl.pallas_call(ffn_kernel, out_shape=jax.ShapeDtypeStruct((n_tok, width),...  117 us

profile of v4, /device:TPU:17, one launch (start us, length us, event | category | flops | bytes accessed | tf_op | source)
XLA Modules:
  0.0 119.2 jit_solution(16184091590650638334)
XLA Ops:
  0.0 116.9 %shard_map.82 = bf16[256,2048]{1,0:T(8,128)(2,1)} custom-call(bf16[256,2048]{1,0:T(8,128)(2,1)} %tok_ref.1, f32[1,2048]{1,0:T(1,128)} %bitcast.6, f32[256,2560]{1,0:T(8,128)} %gate_ref.1, f32[20,128]{1,0:T(8,128)} %bitcast.4, f32[256,2560]{1,0:T(8,128)} %up_ref.1, f32[20,128]{1,0:T(8,128)} %bitcast.5, f32[2560,256]{1,0:T(8,128)} %down_ref.1, f32[1,2048]{1,0:T(1,128)} %bitcast.7), custom_call_target="tpu_custom_call" | custom-call | tf_op jit(solution)/shard_map/pallas_call | solution.py:746
  116.9 2.3 %copy.10 = bf16[256,2048]{1,0:T(8,128)(2,1)} copy(bf16[256,2048]{1,0:T(8,128)(2,1)} %shard_map.82) | data formatting | bytes 2097152

commit v5 on v4

--- a/solution.py
+++ b/solution.py
@@ -66,8 +66,9 @@
 
 
 MESH = pl.DeviceIdType.MESH
-CUTS = 4
+CUTS = 8
 DOWN = 2 * CUTS
+QUARTER = DOWN // 4
 PIECES = 4
 
 
@@ -135,7 +136,7 @@
         return shard_z(turn) * 2 + y + side - 2 * side * y
 
     def z_first(turn, side):
-        return ((turn < 2) & ((side == 1) | (turn + inner == 1))) | ((turn == 2) & (side == 0))
+        return ((turn < 2) & ((side == 1) | (turn + inner == 1))) | ((turn == 3) & (side == 0))
 
     def fold(turn, side):
         block = block_of(turn, side)
@@ -421,9 +422,10 @@
 
             take_y(1, part)
 
-            @pl.when((part == 3) | (part == 5))
-            def _():
-                take_rows((part - 3) // 2)
+            for piece in range(2):
+                @pl.when(part == QUARTER * (piece + 2) - 1)
+                def _():
+                    take_rows(piece)
 
         each(DOWN, second)
         take_rows(2)
@@ -438,13 +440,13 @@
                 take_main(3, part)
                 take_y(2, part)
 
-                @pl.when(part == 3)
+                @pl.when(part == 2 * QUARTER - 1)
                 def _():
                     take_rows(3)
 
-                @pl.when(part > 5)
-                def _():
-                    pass_outward(part - 6)
+                @pl.when(part >= 3 * QUARTER)
+                def _():
+                    pass_outward(part - 3 * QUARTER)
 
             each(DOWN, third)
             y_copy(0, DOWN).start()
@@ -465,8 +467,8 @@
             def fourth(chunk):
                 @pl.when(chunk < 3)
                 def _():
-                    for ahead in (2, 3):
-                        pass_outward(2 * chunk + ahead)
+                    for ahead in range(QUARTER):
+                        pass_outward(QUARTER * (chunk + 1) + ahead)
 
                 @pl.when(chunk == 2)
                 def _():
@@ -475,7 +477,7 @@
 
                 add_early(chunk)
                 add_late(chunk)
-                for part in (2 * chunk, 2 * chunk + 1):
+                for part in [QUARTER * chunk + index for index in range(QUARTER)]:
                     thru_in(3, part).wait_recv()
                     pair_copy(3, part).start()
                     take_y(3, part)
@@ -487,28 +489,28 @@
         @pl.when(is_outer)
         def _():
             def fourth(chunk):
-                for part in (2 * chunk, 2 * chunk + 1):
+                for part in [QUARTER * chunk + index for index in range(QUARTER)]:
                     take_main(2, part)
 
                     @pl.when(chunk > 0)
                     def _():
-                        take_y(2, part - 2)
+                        take_y(2, part - QUARTER)
 
                 add_early(chunk)
 
             each(4, fourth)
 
             def fifth(chunk):
-                for part in (2 * chunk, 2 * chunk + 1):
+                for part in [QUARTER * chunk + index for index in range(QUARTER)]:
                     take_main(3, part)
 
                     @pl.when(chunk == 0)
                     def _():
-                        take_y(2, part + 6)
+                        take_y(2, part + DOWN - QUARTER)
 
                     @pl.when(chunk > 0)
                     def _():
-                        take_y(3, part - 2)
+                        take_y(3, part - QUARTER)
 
                 @pl.when(chunk == 0)
                 def _():
@@ -518,9 +520,11 @@
 
             each(4, fifth)
             c_in(3, 0, 0).wait_recv()
-            take_y(3, 6)
+            for part in range(QUARTER // 2):
+                take_y(3, DOWN - QUARTER + part)
             each(2, add_last)
-            take_y(3, 7)
+            for part in range(QUARTER // 2, QUARTER):
+                take_y(3, DOWN - QUARTER + part)
             each(2, lambda chunk: add_last(chunk + 2))
             take_y(0, DOWN)
             c_in(0, 1, DOWN).wait_recv()
@@ -673,7 +677,7 @@
 
         @pl.when(is_inner)
         def _():
-            late_x(2, 0)
+            late_x(3, 0)
 
         def drain(turns, pair_turns):
             for count, send in ((pair_turns, pair_send), (turns, mid_send)):

time: 119 us -> 118 us (level)
  Pallas kernels: 117 us -> 115 us
    pallas_call x1, Pallas kernels: 117 us -> 115 us  [kernel_body(): pl.pallas_call(ffn_kernel, out_shape=jax.ShapeDtypeStruct((n_tok, width),...]
where the time goes in v5:
time: 118 us; the launch traced here: 117 us
  Pallas kernels  115 us (97%)
  local copies, waits for them, and re-layouts  2.3 us (2%)
    pallas_call x1, Pallas kernels, kernel_body(): pl.pallas_call(ffn_kernel, out_shape=jax.ShapeDtypeStruct((n_tok, width),...  115 us

profile of v5, /device:TPU:17, one launch (start us, length us, event | category | flops | bytes accessed | tf_op | source)
XLA Modules:
  0.0 117.3 jit_solution(2841022420176824059)
XLA Ops:
  0.0 115.0 %shard_map.82 = bf16[256,2048]{1,0:T(8,128)(2,1)} custom-call(bf16[256,2048]{1,0:T(8,128)(2,1)} %tok_ref.1, f32[1,2048]{1,0:T(1,128)} %bitcast.6, f32[256,2560]{1,0:T(8,128)} %gate_ref.1, f32[20,128]{1,0:T(8,128)} %bitcast.4, f32[256,2560]{1,0:T(8,128)} %up_ref.1, f32[20,128]{1,0:T(8,128)} %bitcast.5, f32[2560,256]{1,0:T(8,128)} %down_ref.1, f32[1,2048]{1,0:T(1,128)} %bitcast.7), custom_call_target="tpu_custom_call" | custom-call | tf_op jit(solution)/shard_map/pallas_call | solution.py:750
  115.0 2.3 %copy.10 = bf16[256,2048]{1,0:T(8,128)(2,1)} copy(bf16[256,2048]{1,0:T(8,128)(2,1)} %shard_map.82) | data formatting | bytes 2097152

commit v6 on v5

--- a/solution.py
+++ b/solution.py
@@ -514,6 +514,7 @@
 
                 @pl.when(chunk == 0)
                 def _():
+                    take_y(0, DOWN)
                     c_wait(2)
 
                 add_late(chunk)
@@ -526,7 +527,6 @@
             for part in range(QUARTER // 2, QUARTER):
                 take_y(3, DOWN - QUARTER + part)
             each(2, lambda chunk: add_last(chunk + 2))
-            take_y(0, DOWN)
             c_in(0, 1, DOWN).wait_recv()
 
         def send_off(turn, side, far, near_x):
@@ -563,7 +563,7 @@
             span = pl.ds(pl.multiple_of(near_x * n_tok, n_tok), n_tok)
             pre = []
 
-            @pl.when(index == 1 + inner)
+            @pl.when(index == 1)
             def _():
                 take_main(1, DOWN)
 
@@ -618,7 +618,7 @@
             def _():
                 late_x(0, 0)
 
-            @pl.when(is_inner | (step > 1))
+            @pl.when(step > 1)
             def _():
                 take_y(step - 1, DOWN)
 
@@ -632,6 +632,10 @@
                     def _():
                         late_x(1, 1)
                         take_main(3, DOWN)
+
+                    @pl.when(is_inner & (step == 1) & (side == 1))
+                    def _():
+                        take_y(0, DOWN)
 
                     c_in(turn, side, DOWN).wait_recv()
                     produce(turn, side)

time: 118 us -> 117 us (level)
  no operation moved by 1% of the time
where the time goes in v6:
time: 117 us
  Pallas kernels  115 us (98%)
  local copies, waits for them, and re-layouts  2.3 us (2%)
    pallas_call x1, Pallas kernels, kernel_body(): pl.pallas_call(ffn_kernel, out_shape=jax.ShapeDtypeStruct((n_tok, width),...  115 us

profile of v6, /device:TPU:17, one launch (start us, length us, event | category | flops | bytes accessed | tf_op | source)
XLA Modules:
  0.0 117.3 jit_solution(1873706951832702249)
XLA Ops:
  0.0 115.0 %shard_map.82 = bf16[256,2048]{1,0:T(8,128)(2,1)} custom-call(bf16[256,2048]{1,0:T(8,128)(2,1)} %tok_ref.1, f32[1,2048]{1,0:T(1,128)} %bitcast.6, f32[256,2560]{1,0:T(8,128)} %gate_ref.1, f32[20,128]{1,0:T(8,128)} %bitcast.4, f32[256,2560]{1,0:T(8,128)} %up_ref.1, f32[20,128]{1,0:T(8,128)} %bitcast.5, f32[2560,256]{1,0:T(8,128)} %down_ref.1, f32[1,2048]{1,0:T(1,128)} %bitcast.7), custom_call_target="tpu_custom_call" | custom-call | tf_op jit(solution)/shard_map/pallas_call | solution.py:754
  115.0 2.3 %copy.10 = bf16[256,2048]{1,0:T(8,128)(2,1)} copy(bf16[256,2048]{1,0:T(8,128)(2,1)} %shard_map.82) | data formatting | bytes 2097152
